TPU v7x, 128 devices: a whole 4x4x4 slice. The times are simulated.
128 devices in a mesh: sp: 32 (over z, y, core), tp: 4 (over x).
Axes of the slice: x: 4, y: 4, z: 4, core: 2. Of those that a mesh axis runs over, the one named last changes fastest.
Arguments:
- conv_input: bfloat16 [16384, 1024], P('sp', 'tp'), may hold values from -6 to 6
- gate_inner: bfloat16 [16384, 1024], P('sp', 'tp'), may hold values from -6 to 6
- gate_outer: bfloat16 [16384, 1024], P('sp', 'tp'), may hold values from -6 to 6
- conv_taps: bfloat16 [3, 1024], P(None, 'tp'), may hold values from -3.5 to 3.5
- doc_ids: int32 [16384], P('sp'), may hold values from 0 to 15, never falling along the last dimension, each value on 1 to 2048 neighbouring positions
- residual_in: bfloat16 [16384, 2048], P(('sp', 'tp')), may hold values from -6 to 6
- out_proj: bfloat16 [1024, 2048], replicated, may hold values from -0.1875 to 0.1875
- norm_gain: float32 [2048], replicated, may hold values from 0.1 to 1.9
- expert_ids: int32 [16384, 2], P(('sp', 'tp')), may hold values from 0 to 127, all different within a row; in each aligned block of 128 rows (0 to 127, 128 to 255, ...) at most 4 rows name the same one
- expert_weights: float32 [16384, 2], P(('sp', 'tp')), may hold values from 0.2 to 1
- gate_proj: bfloat16 [128, 2048, 1024], P(('sp', 'tp')), may hold values from -0.125 to 0.125
- up_proj: bfloat16 [128, 2048, 1024], P(('sp', 'tp')), may hold values from -0.125 to 0.125
- down_proj: bfloat16 [128, 1024, 2048], P(('sp', 'tp')), may hold values from -0.1875 to 0.1875
Outputs:
- layer_out: bfloat16 [16384, 2048], P(('sp', 'tp'))
Inputs may be any that keep to these rules, and one draw needn't show every extreme that they name: `doc_ids`: never falls along positions; each document has at most 2048 positions. `expert_ids`: each row names 2 different experts; within the rows of one device, aligned blocks of 128 rows, no expert is named more than 4 times, a bound that some block reaches.
All inputs are finite; a program needn't handle non-finite values.
Results may differ from a plain program's by a relative error of at most 0.009.
Values may be sent and summed in bfloat16 or wider, within the bound.
A program may use at most 64 MiB of HBM per device.

v0:
```python
import jax
import jax.numpy as jnp
from jax import lax
from jax.sharding import PartitionSpec as P


def from_behind(block, axis, distance):
    devices = range(lax.axis_size(axis))
    route = [(i - distance, i) for i in devices if i - distance in devices]
    return lax.ppermute(block, axis, route)


def expert_rows(arrived, gate_weight, up_weight, down_weight):
    gate_value = jnp.dot(arrived, gate_weight, preferred_element_type=jnp.float32)
    up_value = jnp.dot(arrived, up_weight, preferred_element_type=jnp.float32)
    hidden = (jax.nn.silu(gate_value) * up_value).astype(jnp.bfloat16)
    return jnp.dot(hidden, down_weight, preferred_element_type=jnp.float32).astype(jnp.bfloat16)


def on_device(
    conv_input,
    gate_inner,
    gate_outer,
    conv_taps,
    doc_ids,
    residual_in,
    out_proj,
    norm_gain,
    expert_ids,
    expert_weights,
    gate_proj,
    up_proj,
    down_proj,
):
    inner_prod = conv_input.astype(jnp.float32) * gate_inner.astype(jnp.float32)
    earlier, earlier_docs = from_behind((inner_prod[-2:], doc_ids[-2:]), "sp", 1)
    padded = jnp.concatenate([earlier, inner_prod], axis=0)
    padded_docs = jnp.concatenate([earlier_docs, doc_ids], axis=0)
    length = inner_prod.shape[0]
    tap_values = conv_taps.astype(jnp.float32)
    one_back = jnp.where(
        (padded_docs[1 : length + 1] == doc_ids)[:, None], padded[1 : length + 1], 0.0
    )
    two_back = jnp.where((padded_docs[:length] == doc_ids)[:, None], padded[:length], 0.0)
    mixed_rows = tap_values[2] * inner_prod + tap_values[1] * one_back + tap_values[0] * two_back
    conv_out = (gate_outer.astype(jnp.float32) * mixed_rows).astype(jnp.bfloat16)
    row_count = residual_in.shape[0]
    regrouped = lax.all_to_all(conv_out, "tp", split_axis=0, concat_axis=1, tiled=True)
    mix = jnp.dot(regrouped, out_proj, preferred_element_type=jnp.float32).astype(jnp.bfloat16)
    carried = residual_in.astype(jnp.float32) + mix.astype(jnp.float32)
    normed = (
        carried * lax.rsqrt(jnp.mean(carried * carried, axis=1, keepdims=True) + 1e-06) * norm_gain
    ).astype(jnp.bfloat16)
    model_width = normed.shape[1]
    choose = expert_ids.shape[1]
    sp_count = lax.axis_size("sp")
    tp_count = lax.axis_size("tp")
    experts_total = sp_count * tp_count
    capacity = 2 * row_count * choose // experts_total
    flat_ids = expert_ids.reshape(-1)
    onehot = (flat_ids[:, None] == jnp.arange(experts_total, dtype=jnp.int32)[None, :]).astype(
        jnp.int32
    )
    slot_rank = jnp.sum((jnp.cumsum(onehot, axis=0) - 1) * onehot, axis=1)
    target = flat_ids * capacity + slot_rank
    sources = jnp.repeat(normed, choose, axis=0)
    outgoing = (
        jnp.zeros((experts_total * capacity, model_width), jnp.bfloat16).at[target].set(sources)
    )
    gate_weight = gate_proj[0]
    up_weight = up_proj[0]
    down_weight = down_proj[0]
    arrived = lax.all_to_all(
        outgoing.reshape(experts_total, capacity, model_width),
        ("sp", "tp"),
        split_axis=0,
        concat_axis=0,
        tiled=True,
    )
    item_count = arrived.shape[1]
    flat_rows = arrived.reshape(-1, model_width)
    result = expert_rows(flat_rows, gate_weight, up_weight, down_weight)
    result = result.reshape(experts_total, item_count, model_width)
    returned = lax.all_to_all(result, ("sp", "tp"), split_axis=0, concat_axis=0, tiled=True)
    picked = (
        returned.reshape(-1, model_width)[target]
        .reshape(row_count, choose, model_width)
        .astype(jnp.float32)
    )
    combined = carried + jnp.sum(expert_weights[:, :, None] * picked, axis=1)
    return combined.astype(jnp.bfloat16)


def solution(mesh):
    in_specs = (
        P("sp", "tp"),
        P("sp", "tp"),
        P("sp", "tp"),
        P(None, "tp"),
        P("sp"),
        P(("sp", "tp"), None),
        P(),
        P(),
        P(("sp", "tp"), None),
        P(("sp", "tp"), None),
        P(("sp", "tp"), None, None),
        P(("sp", "tp"), None, None),
        P(("sp", "tp"), None, None),
    )
    out_specs = P(("sp", "tp"), None)
    return jax.shard_map(
        on_device, mesh=mesh, in_specs=in_specs, out_specs=out_specs, check_vma=False
    )
```

profile of v0, /device:TPU:1, one launch (start us, length us, event | category | flops | bytes accessed | tf_op | source)
XLA Modules:
  0.0 143.9 jit_solution(9995977291659634800)
XLA Ops:
  0.0 0.0 copy-start.4
  0.0 0.0 copy-start.2
  0.0 0.0 copy-start.1
  0.0 1.2 convert_multiply_fusion
  1.2 4.6 %collective-permute-start.1 = (f32[2,256]{1,0:T(2,128)S(1)}, f32[2,256]{1,0:T(2,128)S(1)}, u32[]{:S(2)}, u32[]{:S(2)}) collective-permute-start(f32[2,256]{1,0:T(2,128)S(1)} %slice.48), channel_id=1, source_target_pairs={{0,4},{4,8},{8,12},{12,16},{16,20},{20,24},{24,28},{28,32},{32,36}... | collective-permute-start | bytes 6152 | tf_op jit(solution)/shard_map/ppermute | solution.py:10
  5.8 0.8 slice.35
  6.5 1.9 %collective-permute-start = (s32[2]{0:T(128)S(1)}, s32[2]{0:T(128)S(1)}, u32[]{:S(2)}, u32[]{:S(2)}) collective-permute-start(s32[2]{0:T(128)S(1)} %slice.35), channel_id=1, source_target_pairs={{0,4},{4,8},{8,12},{12,16},{16,20},{20,24},{24,28},{28,32},{32,36}... | collective-permute-start | bytes 32 | tf_op jit(solution)/shard_map/ppermute | solution.py:10
  8.4 0.8 copy.24
  9.2 0.1 eq.37
  9.4 0.1 eq.33
  9.5 0.7 broadcast_multiply_fusion
  10.2 0.8 fusion.31
  11.0 0.1 copy.26
  11.1 0.2 fusion.26
  11.4 0.1 add_add_fusion
  11.5 0.1 copy.23
  11.6 0.1 mul.103
  11.7 0.2 fusion.27
  11.9 0.0 collective-permute-done
  11.9 0.0 copy-done.4
  11.9 0.1 pad_add_fusion
  12.0 0.1 slice_compare_fusion.1
  12.1 0.0 collective-permute-done.1
  12.1 0.0 copy-done.2
  12.1 1.0 fusion.23
  13.1 4.0 %all-to-all-start = ((bf16[4,128,256]{2,1,0:T(8,128)(2,1)}), bf16[4,128,256]{2,1,0:T(8,128)(2,1)S(1)}, u32[]{:S(2)}, u32[]{:S(2)}) async-start(bf16[4,128,256]{2,1,0:T(8,128)(2,1)} %bitcast.3), calls=%async_computation | async-start | bytes 524288 | tf_op jit(solution)/shard_map/all_to_all | solution.py:48
  17.1 5.7 %all-to-all-done = bf16[4,128,256]{2,1,0:T(8,128)(2,1)S(1)} async-done(((bf16[4,128,256]{2,1,0:T(8,128)(2,1)}), bf16[4,128,256]{2,1,0:T(8,128)(2,1)S(1)}, u32[]{:S(2)}, u32[]{:S(2)}) %all-to-all-start) | async-done | bytes 262176 | tf_op jit(solution)/shard_map/all_to_all | solution.py:48
  22.8 0.2 copy.21
  23.0 0.0 copy-done.1
  23.0 0.0 copy-start.3
  23.0 3.0 %multiply_reduce_fusion.1 = (f32[128]{0:T(128)S(1)}, f32[128,2048]{1,0:T(8,128)S(1)}) fusion(bf16[128,1024]{0,1:T(8,128)(2,1)S(1)} %bitcast.35, bf16[1024,2048]{1,0:T(8,128)(2,1)} %param.19, bf16[128,2048]{1,0:T(8,128)(2,1)S(1)} %copy-done.1), kind=kOutput, calls=%fused_computation.16 | convolution fusion | flops 538443648 | bytes 6029824 | tf_op jit(solution)/shard_map/dot_general | solution.py:49
  26.0 0.0 copy-done.3
  26.0 0.2 multiply_convert_fusion.1
  26.2 0.6 broadcast_in_dim.36
  26.8 1.2 reshape.100
  28.1 3.5 %scatter_custom_fusion = bf16[512,2048]{1,0:T(8,128)(2,1)S(1)} fusion(s32[256]{0:T(256)S(1)} %bitcast.38, bf16[256,2048]{1,0:T(8,128)(2,1)} %reshape.100, bf16[]{:T(256)} %constant.6.clone.1), kind=kCustom, calls=%fused_computation.17 | custom fusion | bytes 2097664 | tf_op jit(solution)/shard_map/scatter | solution.py:68
  31.6 2.2 %reshape.83 = bf16[128,4,2048]{2,1,0:T(4,128)(2,1)} reshape(bf16[512,2048]{1,0:T(8,128)(2,1)S(1)} %scatter_custom_fusion) | data formatting | bytes 4194304 | tf_op jit(solution)/shard_map/reshape | solution.py:74
  33.8 40.5 %all_to_all.29 = bf16[128,4,2048]{2,1,0:T(4,128)(2,1)S(1)} all-to-all(bf16[128,4,2048]{2,1,0:T(4,128)(2,1)} %reshape.83), channel_id=1, replica_groups=mesh['sp'=32,'tp'=4] {'sp','tp'}, dimensions={0} | all-to-all | bytes 4194304 | tf_op jit(solution)/shard_map/all_to_all | solution.py:73
  74.3 2.0 %reshape.84 = bf16[512,2048]{1,0:T(8,128)(2,1)} reshape(bf16[128,4,2048]{2,1,0:T(4,128)(2,1)S(1)} %all_to_all.29) | data formatting | bytes 4194304 | tf_op jit(solution)/shard_map/reshape | solution.py:81
  76.4 0.0 copy-start
  76.4 6.6 %fusion.4 = f32[512,1024]{1,0:T(8,128)} fusion(bf16[512,2048]{1,0:T(8,128)(2,1)} %reshape.84, bf16[1,2048,1024]{2,1,0:T(8,128)(2,1)} %param.23), kind=kOutput, calls=%fused_computation.6 | convolution fusion | flops 2147483648 | bytes 8388608 | tf_op jit(solution)/shard_map/dot_general | solution.py:14
  83.0 0.0 copy-done
  83.0 9.9 %fusion.6 = bf16[512,2048]{1,0:T(8,128)(2,1)} fusion(bf16[1,1024,2048]{2,1,0:T(8,128)(2,1)} %param.25, f32[512,1024]{1,0:T(8,128)} %fusion.4, bf16[512,2048]{1,0:T(8,128)(2,1)S(1)} %copy-done, bf16[1,2048,1024]{2,1,0:T(8,128)(2,1)} %param.24), kind=kOutput, calls=%fused_computation.8 | convolution fusion | flops 4299161600 | bytes 14680064 | tf_op jit(solution)/shard_map/dot_general | solution.py:17
  92.9 4.1 %reshape.85 = bf16[128,4,2048]{2,1,0:T(4,128)(2,1)} reshape(bf16[512,2048]{1,0:T(8,128)(2,1)} %fusion.6) | data formatting | bytes 4194304 | tf_op jit(solution)/shard_map/reshape | solution.py:83
  97.0 0.0 copy-start.5
  97.0 5.0 %all-to-all-start.2 = ((bf16[128,4,2048]{2,1,0:T(4,128)(2,1)}), bf16[128,4,2048]{2,1,0:T(4,128)(2,1)}, u32[]{:S(2)}, u32[]{:S(2)}) async-start(bf16[128,4,2048]{2,1,0:T(4,128)(2,1)} %reshape.85), calls=%async_computation.2 | async-start | bytes 4194304 | tf_op jit(solution)/shard_map/all_to_all | solution.py:84
  102.0 0.0 copy-done.5
  102.0 0.1 copy.22
  102.1 30.4 %all-to-all-done.2 = bf16[128,4,2048]{2,1,0:T(4,128)(2,1)} async-done(((bf16[128,4,2048]{2,1,0:T(4,128)(2,1)}), bf16[128,4,2048]{2,1,0:T(4,128)(2,1)}, u32[]{:S(2)}, u32[]{:S(2)}) %all-to-all-start.2) | async-done | bytes 2097184 | tf_op jit(solution)/shard_map/all_to_all | solution.py:84
  132.6 2.5 %reshape.86 = bf16[512,2048]{1,0:T(8,128)(2,1)S(1)} reshape(bf16[128,4,2048]{2,1,0:T(4,128)(2,1)} %all-to-all-done.2) | data formatting | bytes 4194304 | tf_op jit(solution)/shard_map/reshape | solution.py:86
  135.1 2.3 %gather_fusion = bf16[256,2048]{1,0:T(8,128)(2,1)} fusion(bf16[512,2048]{1,0:T(8,128)(2,1)S(1)} %reshape.86, s32[1024]{0:T(1024)S(1)} %pad_clamp_fusion), kind=kCustom, calls=%fused_computation | custom fusion | bytes 2098176 | tf_op jit(solution)/shard_map/gather | solution.py:86
  137.4 2.4 %reshape.87 = f32[128,2,2048]{2,1,0:T(2,128)S(1)} reshape(bf16[256,2048]{1,0:T(8,128)(2,1)} %gather_fusion) | data formatting | bytes 3145728 | tf_op jit(solution)/shard_map/convert_element_type | solution.py:88
  139.8 3.2 %multiply_reduce_fusion = f32[128,2048]{1,0:T(8,128)S(1)} fusion(f32[128,2,2048]{2,1,0:T(2,128)S(1)} %reshape.87, f32[128,2]{1,0:T(8,128)S(1)} %copy.22), kind=kLoop, calls=%fused_computation.12 | loop fusion | flops 786432 | bytes 3146752 | tf_op jit(solution)/shard_map/reduce_sum | solution.py:90
  143.0 0.9 add_convert_fusion
  (8 shorter events, 0.1 us)
Async XLA Ops:
  0.0 11.9 %copy-start.4 = (s32[512]{0:T(512)S(1)}, s32[512]{0:T(512)}, u32[]{:S(2)}) copy-start(s32[512]{0:T(512)} %param.17) | copy-start | bytes 6148
  0.0 12.1 %copy-start.2 = (bf16[512,256]{1,0:T(8,128)(2,1)S(1)}, bf16[512,256]{1,0:T(8,128)(2,1)}, u32[]{:S(2)}) copy-start(bf16[512,256]{1,0:T(8,128)(2,1)} %param.15) | copy-start | bytes 786436
  0.0 23.0 %copy-start.1 = (bf16[128,2048]{1,0:T(8,128)(2,1)S(1)}, bf16[128,2048]{1,0:T(8,128)(2,1)}, u32[]{:S(2)}) copy-start(bf16[128,2048]{1,0:T(8,128)(2,1)} %param.18) | copy-start | bytes 1572868
  1.2 10.9 %collective-permute-start.1 = (f32[2,256]{1,0:T(2,128)S(1)}, f32[2,256]{1,0:T(2,128)S(1)}, u32[]{:S(2)}, u32[]{:S(2)}) collective-permute-start(f32[2,256]{1,0:T(2,128)S(1)} %slice.48), channel_id=1, source_target_pairs={{0,4},{4,8},{8,12},{12,16},{16,20},{20,24},{24,28},{28,32},{32,36}... | collective-permute-start | bytes 6152 | tf_op jit(solution)/shard_map/ppermute | solution.py:10
  6.5 5.4 %collective-permute-start = (s32[2]{0:T(128)S(1)}, s32[2]{0:T(128)S(1)}, u32[]{:S(2)}, u32[]{:S(2)}) collective-permute-start(s32[2]{0:T(128)S(1)} %slice.35), channel_id=1, source_target_pairs={{0,4},{4,8},{8,12},{12,16},{16,20},{20,24},{24,28},{28,32},{32,36}... | collective-permute-start | bytes 32 | tf_op jit(solution)/shard_map/ppermute | solution.py:10
  13.1 9.7 %all-to-all-start = ((bf16[4,128,256]{2,1,0:T(8,128)(2,1)}), bf16[4,128,256]{2,1,0:T(8,128)(2,1)S(1)}, u32[]{:S(2)}, u32[]{:S(2)}) async-start(bf16[4,128,256]{2,1,0:T(8,128)(2,1)} %bitcast.3), calls=%async_computation | async-start | bytes 524288 | tf_op jit(solution)/shard_map/all_to_all | solution.py:48
  23.0 3.0 %copy-start.3 = (f32[2048]{0:T(1024)S(1)}, f32[2048]{0:T(1024)}, u32[]{:S(2)}) copy-start(f32[2048]{0:T(1024)} %param.20) | copy-start | bytes 24580
  76.4 6.7 %copy-start = (bf16[512,2048]{1,0:T(8,128)(2,1)S(1)}, bf16[512,2048]{1,0:T(8,128)(2,1)}, u32[]{:S(2)}) copy-start(bf16[512,2048]{1,0:T(8,128)(2,1)} %reshape.84) | copy-start | bytes 6291460
  97.0 5.0 %copy-start.5 = (f32[128,2]{0,1:T(2,128)S(1)}, f32[128,2]{0,1:T(2,128)}, u32[]{:S(2)}) copy-start(f32[128,2]{0,1:T(2,128)} %param.22) | copy-start | bytes 3076
  97.0 35.5 %all-to-all-start.2 = ((bf16[128,4,2048]{2,1,0:T(4,128)(2,1)}), bf16[128,4,2048]{2,1,0:T(4,128)(2,1)}, u32[]{:S(2)}, u32[]{:S(2)}) async-start(bf16[128,4,2048]{2,1,0:T(4,128)(2,1)} %reshape.85), calls=%async_computation.2 | async-start | bytes 4194304 | tf_op jit(solution)/shard_map/all_to_all | solution.py:84
where the time goes:
time: 145 us; the launch traced here: 144 us
  blocking collectives  40.5 us (28%)
  waiting for transfers between devices  36.1 us (25%)
  local copies, waits for them, and re-layouts  24.3 us (17%)
  matrix products  19.6 us (14%)
  starting transfers between devices  15.5 us (11%)
  other arithmetic  7.76 us (5%)
    all_to_all x1, blocking collectives, on_device(): lax.all_to_all(outgoing.reshape(experts_total, capacity, model_width), ('...  40.5 us
    all_to_all x1, waiting for transfers between devices, on_device(): lax.all_to_all(result, ('sp', 'tp'), split_axis=0, concat_axis=0, tiled=T...  30.4 us
    dot_general x1, matrix products, expert_rows(): jnp.dot(hidden, down_weight, preferred_element_type=jnp.float32)  9.9 us
    dot_general x1, matrix products, expert_rows(): jnp.dot(arrived, gate_weight, preferred_element_type=jnp.float32)  6.65 us
    ppermute x2, starting transfers between devices, from_behind(): return lax.ppermute(block, axis, route)  6.49 us
    all_to_all x1, waiting for transfers between devices, on_device(): lax.all_to_all(conv_out, 'tp', split_axis=0, concat_axis=1, tiled=True)  5.69 us
    all_to_all x1, starting transfers between devices, on_device(): lax.all_to_all(result, ('sp', 'tp'), split_axis=0, concat_axis=0, tiled=T...  4.97 us
    reshape x1, local copies, waits for them, and re-layouts, on_device(): result = result.reshape(experts_total, item_count, model_width)  4.11 us
  transfers between devices with their start and end apart: 4, of which 2 were waited for; matrix products, arithmetic and copies ran while one was open for 3% of the time, Pallas kernels for 0%

commit v1 on v0

v1 whole, which is shorter than its diff:
```python
import jax
import jax.numpy as jnp
from jax import lax
from jax.experimental import pallas as pl
from jax.experimental.pallas import tpu as pltpu
from jax.sharding import PartitionSpec as P

MESH = pl.DeviceIdType.MESH
BF = jnp.bfloat16
F32 = jnp.float32
NCH = 16
W = 128
HALF = (2,) * 5 + (8, W)
CUBE = (2,) * 6 + (8, W)


def gray_bits(v):
    return [(v // 2 + v % 2) % 2, v // 2]


def gray_flip(v, bit):
    return v + 1 - 2 * (v % 2) if bit == 0 else 3 - v


def layer_kernel(
    ci_h, gi_h, go_h, taps, docs, res_h, op_h, gain, ids, wts, wg_h, wu_h, wd_h,
    out,
    ci, gi, go, res, opv, wg, wu, wd,
    inner, halo, dhalo, docs8, conv_send, conv_all,
    carried, meta_send, meta, tok, pack, a_buf, land, gsum, usum, hid, y_buf, land2, comb,
    part_send, part_recv,
    load_sem, misc_send, misc_recv, tp_send, tp_recv, tok_send, tok_recv,
    d_send, d_recv, c_send, c_recv, p_send, p_recv,
):
    sp = lax.axis_index("sp")
    x = lax.axis_index("tp")
    c = sp % 2
    y = (sp // 2) % 4
    z = sp // 8
    mine = gray_bits(x) + gray_bits(y) + gray_bits(z)

    def neighbour(d):
        xx, yy, zz = x, y, z
        if d < 2:
            xx = gray_flip(x, d)
        elif d < 4:
            yy = gray_flip(y, d - 2)
        else:
            zz = gray_flip(z, d - 4)
        return ((zz * 4 + yy) * 2 + c, xx)

    nbr = [neighbour(d) for d in range(6)]
    twin = (sp + 1 - 2 * c, x)
    after = ((sp + 1) % 32, x)
    before = ((sp + 31) % 32, x)
    tp_far = [(sp, (x + j) % 4) for j in range(4)]

    def load(src, dst, i):
        return pltpu.make_async_copy(src, dst, load_sem.at[i])

    loads = [load(ci_h, ci, 0), load(gi_h, gi, 1), load(go_h, go, 2), load(res_h, res, 3),
             load(op_h, opv, 4), load(wg_h.at[0], wg, 5), load(wu_h.at[0], wu, 6), load(wd_h.at[0], wd, 7)]
    for i in range(3):
        loads[i].start()

    bar = pltpu.get_barrier_semaphore()
    for dev in nbr + [twin, tp_far[2], after, before]:
        pl.semaphore_signal(bar, inc=1, device_id=dev, device_id_type=MESH)

    meta_send[0:2, :] = ids[...].astype(F32)
    meta_send[2:4, :] = wts[...]
    docs8[1:5, :] = docs[...]

    for i in range(2):
        loads[i].wait()
    inner[8:520, :] = ci[...].astype(F32) * gi[...].astype(F32)
    loads[2].wait()
    for i in range(3, 8):
        loads[i].start()

    def remote(src, dst, ssem, rsem, dev):
        return pltpu.make_async_remote_copy(
            src_ref=src, dst_ref=dst, send_sem=ssem, recv_sem=rsem, device_id=dev, device_id_type=MESH
        )

    pl.semaphore_wait(bar, 10)
    halo_copy = remote(inner.at[pl.ds(512, 8)], halo, misc_send.at[0], misc_recv.at[0], after)
    doc_copy = remote(docs, dhalo, misc_send.at[1], misc_recv.at[1], after)
    meta_copy = remote(meta_send, meta, misc_send.at[2], misc_recv.at[2], twin)
    halo_copy.start()
    doc_copy.start()
    meta_copy.start()

    rows = lax.broadcasted_iota(jnp.int32, (128, 128), 0)
    lanes = lax.broadcasted_iota(jnp.int32, (128, 128), 1)
    eye = jnp.where(rows == lanes, 1.0, 0.0).astype(F32)

    def column(row):
        return jnp.sum(eye * row, axis=1, keepdims=True)

    t0 = taps[0:1, :].astype(F32)
    t1 = taps[1:2, :].astype(F32)
    t2 = taps[2:3, :].astype(F32)
    lane8 = lax.broadcasted_iota(jnp.int32, (8, 128), 1)

    def conv_block(b):
        cur = jnp.broadcast_to(docs8[b + 1 : b + 2, :], (8, 128))
        prev = jnp.broadcast_to(docs8[b : b + 1, :], (8, 128))
        one = jnp.where(lane8 < 1, pltpu.roll(prev, 1, 1), pltpu.roll(cur, 1, 1))
        two = jnp.where(lane8 < 2, pltpu.roll(prev, 2, 1), pltpu.roll(cur, 2, 1))
        m1 = column(jnp.where(one == cur, 1.0, 0.0).astype(F32)[0:1, :])
        m2 = column(jnp.where(two == cur, 1.0, 0.0).astype(F32)[0:1, :])
        base = 8 + 128 * b
        i0 = inner[base : base + 128, :]
        i1 = inner[base - 1 : base + 127, :]
        i2 = inner[base - 2 : base + 126, :]
        value = t2 * i0 + t1 * (m1 * i1) + t0 * (m2 * i2)
        gate = go[128 * b : 128 * b + 128, :].astype(F32)
        conv_send[b] = (gate * value).astype(BF)

    def tp_copy(b):
        slot = (b + 4 - x) % 4
        return remote(conv_send.at[b], conv_all.at[x], tp_send.at[slot], tp_recv.at[slot], (sp, b))

    for b in (1, 2, 3, 0):
        if b == 0:
            halo_copy.wait_recv()
            doc_copy.wait_recv()
            inner[0:8, :] = halo[...]
            docs8[0:1, :] = jnp.where(sp == 0, -1, dhalo[3:4, :])
        conv_block(b)

        @pl.when(x != b)
        def _():
            tp_copy(b).start()

        @pl.when(x == b)
        def _():
            conv_all[b] = conv_send[b]

    meta_copy.wait_recv()

    def routing(table):
        e = [table[a : a + 1, :] for a in range(2)]
        ec = [column(v) for v in e]
        out_rows = []
        for a in range(2):
            same = ((ec[0] == e[a]) | (ec[1] == e[a])) & (rows < lanes)
            rank = jnp.sum(jnp.where(same, 1.0, 0.0).astype(F32), axis=0, keepdims=True)
            ei = e[a].astype(jnp.int32)

            def gray(v):
                return v ^ (v >> 1)

            unit = gray(ei & 3) + 4 * gray((ei >> 3) & 3) + 16 * gray((ei >> 5) & 3)
            out_rows.append((unit * 8 + rank.astype(jnp.int32), (ei >> 2) & 1))
        return out_rows

    slot_rows = lax.broadcasted_iota(jnp.int32, (512, 128), 0)
    slot_lanes = lax.broadcasted_iota(jnp.int32, (128, 512), 1).astype(F32)
    for s, table in ((0, meta_send), (1, meta)):
        source_core = c if s == 0 else 1 - c
        targets = []
        for slot, parity in routing(table):
            targets.append(jnp.where(parity == c, slot + 4 * source_core, -1))
        hit = (slot_rows == targets[0]) | (slot_rows == targets[1])
        pack[:, 128 * s : 128 * s + 128] = jnp.where(hit, 1.0, 0.0).astype(F32).astype(BF)
        weight = jnp.zeros((128, 512), F32)
        for a in range(2):
            tc = column(targets[a].astype(F32))
            wc = column(table[2 + a : 3 + a, :])
            weight = weight + jnp.where(slot_lanes == tc, wc, 0.0)
        high = weight.astype(BF)
        comb[0, 128 * s : 128 * s + 128, :] = high
        comb[1, 128 * s : 128 * s + 128, :] = (weight - high.astype(F32)).astype(BF)

    loads[3].wait()
    loads[4].wait()
    for j in range(1, 4):
        pltpu.make_async_remote_copy(
            src_ref=conv_send.at[0], dst_ref=conv_all.at[(x + 4 - j) % 4], send_sem=tp_send.at[j],
            recv_sem=tp_recv.at[j], device_id=tp_far[j], device_id_type=MESH,
        ).wait_recv()
    total = jnp.zeros((128, 1), F32)
    for n in range(8):
        cols = slice(256 * n, 256 * n + 256)
        acc = jnp.zeros((128, 256), F32)
        for i in range(4):
            acc = acc + jnp.dot(conv_all[i], opv[256 * i : 256 * i + 256, cols], preferred_element_type=F32)
        value = res[:, cols].astype(F32) + acc.astype(BF).astype(F32)
        total = total + jnp.sum(value * value, axis=1, keepdims=True)
        carried[2 * n] = value[:, :128]
        carried[2 * n + 1] = value[:, 128:]
    scale = lax.rsqrt(total / 2048.0 + 1e-6)

    def tok_copy(j):
        ks = pl.ds(4 * j, 4)
        return remote(tok.at[ks, pl.ds(0, 128)], tok.at[ks, pl.ds(128, 128)], tok_send.at[j], tok_recv.at[j], twin)

    for k in range(NCH):
        tok[k, 0:128, :] = (carried[k] * scale * gain[:, W * k : W * k + W]).astype(BF)
        if k % 4 == 3:
            tok_copy(k // 4).start()

    def bit_view(buf, k, d, v):
        index = [slice(None)] * 6
        index[5 - d] = v
        return buf.at[(k, *index)]

    def swap(buf, landing, ss, rs, p, k):
        d = (k + p) % 6
        return remote(bit_view(buf, k, d, 1 - mine[d]), landing.at[d, k], ss.at[d, k], rs.at[d, k], nbr[d])

    def settle(buf, landing, ss, rs, p, k):
        d = (k + p) % 6
        copy = swap(buf, landing, ss, rs, p, k)
        copy.wait_recv()
        copy.wait_send()
        view = bit_view(buf, k, d, 1 - mine[d])
        view[...] = landing[d, k]

    def put(buf, k, value):
        buf[k] = value.reshape(CUBE).astype(BF)

    def pair(buf, k):
        both = [buf[k + i].astype(F32).reshape(512, W).astype(BF) for i in range(2)]
        return jnp.concatenate(both, axis=1)

    for k in range(0, NCH, 2):
        if k % 4 == 0:
            tok_copy(k // 4).wait_recv()
        source = jnp.concatenate([tok[k], tok[k + 1]], axis=1)
        packed = jnp.dot(pack[...], source, preferred_element_type=F32)
        for i in range(2):
            put(a_buf, k + i, packed[:, W * i : W * i + W])
            swap(a_buf, land, d_send, d_recv, 0, k + i).start()

    for p in range(1, 6):
        for k in range(NCH):
            settle(a_buf, land, d_send, d_recv, p - 1, k)
            swap(a_buf, land, d_send, d_recv, p, k).start()

    loads[5].wait()
    loads[6].wait()
    for k in range(0, NCH, 2):
        settle(a_buf, land, d_send, d_recv, 5, k)
        settle(a_buf, land, d_send, d_recv, 5, k + 1)
        source = pair(a_buf, k)
        rows_k = slice(W * k, W * k + 2 * W)
        for n in range(0, 1024, 512):
            g = jnp.dot(source, wg[rows_k, n : n + 512], preferred_element_type=F32)
            u = jnp.dot(source, wu[rows_k, n : n + 512], preferred_element_type=F32)
            if k == 0:
                gsum[:, n : n + 512] = g
                usum[:, n : n + 512] = u
            else:
                gsum[:, n : n + 512] += g
                usum[:, n : n + 512] += u

    @pl.loop(0, 16)
    def _(r):
        rs = pl.ds(pl.multiple_of(r * 32, 32), 32)
        g = gsum[rs, :]
        hid[rs, :] = (g / (1.0 + jnp.exp(-g)) * usum[rs, :]).astype(BF)

    loads[7].wait()
    for k in range(0, NCH, 2):
        result = jnp.dot(hid[...], wd[:, W * k : W * k + 2 * W], preferred_element_type=F32)
        for i in range(2):
            put(y_buf, k + i, result[:, W * i : W * i + W])
            swap(y_buf, land2, c_send, c_recv, 0, k + i).start()

    for p in range(1, 6):
        for k in range(NCH):
            settle(y_buf, land2, c_send, c_recv, p - 1, k)
            swap(y_buf, land2, c_send, c_recv, p, k).start()

    def part_copy(k):
        return remote(part_send.at[k], part_recv.at[k], p_send.at[k], p_recv.at[k], twin)

    for k in range(0, NCH, 2):
        settle(y_buf, land2, c_send, c_recv, 5, k)
        settle(y_buf, land2, c_send, c_recv, 5, k + 1)
        source = pair(y_buf, k)
        both = jnp.dot(comb[0], source, preferred_element_type=F32) + jnp.dot(
            comb[1], source, preferred_element_type=F32
        )
        for i in range(2):
            cols = slice(W * i, W * i + W)
            part_send[k + i] = both[128:, cols]
            part_copy(k + i).start()
            carried[k + i] += both[:128, cols]

    for k in range(NCH):
        part_copy(k).wait_recv()
        out[:, W * k : W * k + W] = (carried[k] + part_recv[k]).astype(BF)

    halo_copy.wait_send()
    doc_copy.wait_send()
    meta_copy.wait_send()
    for j in range(1, 4):
        pltpu.make_async_remote_copy(
            src_ref=conv_send.at[0], dst_ref=conv_all.at[0], send_sem=tp_send.at[j],
            recv_sem=tp_recv.at[j], device_id=tp_far[j], device_id_type=MESH,
        ).wait_send()
    for j in range(4):
        tok_copy(j).wait_send()
    for k in range(NCH):
        part_copy(k).wait_send()


def on_device(ci, gi, go, taps, docs, res, op, gain, ids, wts, wg, wu, wd):
    vmem = pl.BlockSpec(memory_space=pltpu.VMEM)
    hbm = pl.BlockSpec(memory_space=pl.ANY)
    dma = pltpu.SemaphoreType.DMA
    scratch = [
        pltpu.VMEM((512, 256), BF), pltpu.VMEM((512, 256), BF), pltpu.VMEM((512, 256), BF),
        pltpu.VMEM((128, 2048), BF), pltpu.VMEM((1024, 2048), BF),
        pltpu.VMEM((2048, 1024), BF), pltpu.VMEM((2048, 1024), BF), pltpu.VMEM((1024, 2048), BF),
        pltpu.VMEM((520, 256), F32), pltpu.VMEM((8, 256), F32), pltpu.VMEM((4, 128), jnp.int32),
        pltpu.VMEM((8, 128), jnp.int32), pltpu.VMEM((4, 128, 256), BF), pltpu.VMEM((4, 128, 256), BF),
        pltpu.VMEM((NCH, 128, W), F32), pltpu.VMEM((4, 128), F32), pltpu.VMEM((4, 128), F32),
        pltpu.VMEM((NCH, 256, W), BF), pltpu.VMEM((512, 256), BF),
        pltpu.VMEM((NCH, *CUBE), BF), pltpu.VMEM((6, NCH, *HALF), BF),
        pltpu.VMEM((512, 1024), F32), pltpu.VMEM((512, 1024), F32), pltpu.VMEM((512, 1024), BF),
        pltpu.VMEM((NCH, *CUBE), BF), pltpu.VMEM((6, NCH, *HALF), BF), pltpu.VMEM((2, 256, 512), BF),
        pltpu.VMEM((NCH, 128, W), F32), pltpu.VMEM((NCH, 128, W), F32),
        dma((8,)), dma((3,)), dma((3,)), dma((4,)), dma((4,)), dma((4,)), dma((4,)),
        dma((6, NCH)), dma((6, NCH)), dma((6, NCH)), dma((6, NCH)), dma((NCH,)), dma((NCH,)),
    ]
    return pl.pallas_call(
        layer_kernel,
        out_shape=jax.ShapeDtypeStruct((128, 2048), BF),
        in_specs=[hbm, hbm, hbm, vmem, vmem, hbm, hbm, vmem, vmem, vmem, hbm, hbm, hbm],
        out_specs=vmem,
        scratch_shapes=scratch,
        compiler_params=pltpu.CompilerParams(
            collective_id=0, has_side_effects=True, vmem_limit_bytes=64000000
        ),
    )(ci, gi, go, taps, docs.reshape(4, 128), res, op, gain.reshape(1, 2048), ids.T, wts.T, wg, wu, wd)


def solution(mesh):
    in_specs = (
        P("sp", "tp"),
        P("sp", "tp"),
        P("sp", "tp"),
        P(None, "tp"),
        P("sp"),
        P(("sp", "tp"), None),
        P(),
        P(),
        P(("sp", "tp"), None),
        P(("sp", "tp"), None),
        P(("sp", "tp"), None, None),
        P(("sp", "tp"), None, None),
        P(("sp", "tp"), None, None),
    )
    out_specs = P(("sp", "tp"), None)
    return jax.shard_map(
        on_device, mesh=mesh, in_specs=in_specs, out_specs=out_specs, check_vma=False
    )
```

time: 145 us -> 89.6 us (0.62)
  Pallas kernels: 0 us -> 87.4 us
  blocking collectives: 40.5 us -> 0 us
  waiting for transfers between devices: 36.1 us -> 0 us
  local copies, waits for them, and re-layouts: 24.3 us -> 1.88 us
  matrix products: 19.6 us -> 0 us
  starting transfers between devices: 15.5 us -> 0 us
  other arithmetic: 7.76 us -> 0 us
    pallas_call x0 -> x1, Pallas kernels: none -> 87.4 us  [on_device(): pl.pallas_call(layer_kernel, out_shape=jax.ShapeDtypeStruct((128, 2048),...]
    all_to_all x1 -> x0, blocking collectives: 40.5 us -> none  [on_device(): lax.all_to_all(outgoing.reshape(experts_total, capacity, model_width), ('...]
    all_to_all x2 -> x0, waiting for transfers between devices: 36.1 us -> none  [the longest x1 30.4 us: on_device(): lax.all_to_all(result, ('sp', 'tp'), split_axis=0, concat_axis=0, tiled=T...]
    dot_general x3 -> x0, matrix products: 19.6 us -> none  [the longest x1 9.9 us: expert_rows(): jnp.dot(hidden, down_weight, preferred_element_type=jnp.float32)]
    reshape x5 -> x0, local copies, waits for them, and re-layouts: 12.1 us -> none  [the longest x1 4.11 us: on_device(): result = result.reshape(experts_total, item_count, model_width)]
    all_to_all x2 -> x0, starting transfers between devices: 8.99 us -> none  [the longest x1 4.97 us: on_device(): lax.all_to_all(result, ('sp', 'tp'), split_axis=0, concat_axis=0, tiled=T...]
    ppermute x2 -> x0, starting transfers between devices: 6.49 us -> none  [from_behind(): return lax.ppermute(block, axis, route)]
    scatter x1 -> x0, local copies, waits for them, and re-layouts: 3.5 us -> none  [on_device(): jnp.zeros((experts_total * capacity, model_width), jnp.bfloat16).at[target]]
  transfers between devices with their start and end apart: 4 -> 0, of which waited for: 2 -> 0; matrix products, arithmetic and copies ran while one was open for 3% -> 0% of each run, Pallas kernels for 0% -> 0%
where the time goes in v1:
time: 89.6 us; the launch traced here: 89.3 us
  Pallas kernels  87.4 us (98%)
  local copies, waits for them, and re-layouts  1.88 us (2%)
    pallas_call x1, Pallas kernels, on_device(): pl.pallas_call(layer_kernel, out_shape=jax.ShapeDtypeStruct((128, 2048),...  87.4 us
    unnamed x1, local copies, waits for them, and re-layouts  1.88 us

profile of v1, /device:TPU:1, one launch (start us, length us, event | category | flops | bytes accessed | tf_op | source)
XLA Modules:
  0.0 89.3 jit_solution(5807169516511610846)
XLA Ops:
  0.0 87.4 %shard_map.127 = bf16[128,2048]{1,0:T(8,128)(2,1)} custom-call(bf16[512,256]{1,0:T(8,128)(2,1)} %ci_h.1, bf16[512,256]{1,0:T(8,128)(2,1)} %gi_h.1, bf16[512,256]{1,0:T(8,128)(2,1)} %go_h.1, bf16[3,256]{1,0:T(4,128)(2,1)} %taps.1, s32[4,128]{1,0:T(4,128)} %bitcast.5, bf16[128,2048]{1,0:T(8,128)(2,1)} %res_h.1, bf16[1024,2048]{1,0:T(8,128)(2,1)} %op_h.1, ...), custom_call_target="tpu_custom_call" | custom-call | tf_op jit(solution)/shard_map/pallas_call | solution.py:331
  87.5 1.9 %copy.15 = bf16[128,2048]{1,0:T(8,128)(2,1)} copy(bf16[128,2048]{1,0:T(8,128)(2,1)} %shard_map.127) | data formatting | bytes 1048576

commit v2 on v1

v2 whole, which is shorter than its diff:
```python
import jax
import jax.numpy as jnp
from jax import lax
from jax.experimental import pallas as pl
from jax.experimental.pallas import tpu as pltpu
from jax.sharding import PartitionSpec as P

MESH = pl.DeviceIdType.MESH
BF = jnp.bfloat16
F32 = jnp.float32
NCH = 8
W = 256
CUBE = (4, 4, 4, 8, W)
STEPS = (2, 1, 3)


def layer_kernel(
    ci_h, gi_h, go_h, taps, docs, res_h, op_h, gain, ids, wts, wg_h, wu_h, wd_h,
    out,
    ci, gi, go, res, opv, wg, wu, wd,
    inner, halo_send, halo_all, fix_send, fix_all, docs8, conv_send, conv_all,
    carried, meta_send, meta, tok, pack, there, gsum, usum, hid, back, comb,
    part_send, part_recv,
    load_sem, halo_s, halo_r, fix_s, fix_r, meta_s, meta_r, tp_send, tp_recv, tok_send, tok_recv,
    d_send, d_recv, c_send, c_recv, p_send, p_recv,
):
    sp = lax.axis_index("sp")
    x = lax.axis_index("tp")
    c = sp % 2
    y = (sp // 2) % 4
    z = sp // 8
    here = [z, y, x]

    def along(axis, step):
        at = [z, y, x]
        at[axis] = (at[axis] + step) % 4
        return ((at[0] * 4 + at[1]) * 2 + c, at[2])

    twin = (sp + 1 - 2 * c, x)
    after = ((sp + 1) % 32, 0)
    tp_far = [(sp, (x + j) % 4) for j in range(4)]

    def load(src, dst, i):
        return pltpu.make_async_copy(src, dst, load_sem.at[i])

    loads = [load(ci_h, ci, 0), load(gi_h, gi, 1), load(go_h, go, 2), load(res_h, res, 3),
             load(op_h, opv, 4), load(wg_h.at[0], wg, 5), load(wu_h.at[0], wu, 6), load(wd_h.at[0], wd, 7)]
    for i in range(3):
        loads[i].start()

    bar = pltpu.get_barrier_semaphore()
    for axis in range(3):
        for step in STEPS:
            pl.semaphore_signal(bar, inc=1, device_id=along(axis, step), device_id_type=MESH)
    pl.semaphore_signal(bar, inc=1, device_id=twin, device_id_type=MESH)

    @pl.when(x == 0)
    def _():
        for t in range(4):
            pl.semaphore_signal(bar, inc=1, device_id=((sp + 31) % 32, t), device_id_type=MESH)

    meta_send[0:2, :] = ids[...].astype(F32)
    meta_send[2:4, :] = wts[...]
    docs8[0:1, :] = jnp.full((1, 128), -1, jnp.int32)
    docs8[1:5, :] = docs[...]
    inner[0:8, :] = jnp.zeros((8, 256), F32)

    for i in range(2):
        loads[i].wait()
    inner[8:520, :] = ci[...].astype(F32) * gi[...].astype(F32)
    loads[2].wait()
    for i in range(3, 8):
        loads[i].start()

    def remote(src, dst, ssem, rsem, dev):
        return pltpu.make_async_remote_copy(
            src_ref=src, dst_ref=dst, send_sem=ssem, recv_sem=rsem, device_id=dev, device_id_type=MESH
        )

    t0 = taps[0:1, :].astype(F32)
    t1 = taps[1:2, :].astype(F32)
    t2 = taps[2:3, :].astype(F32)
    last = docs[3:4, :].astype(F32)
    halo_send[0:1, :] = t1 * inner[519:520, :]
    halo_send[1:2, :] = t0 * inner[518:519, :]
    halo_send[2:3, :] = t0 * inner[519:520, :]
    halo_send[3:4, :] = jnp.broadcast_to(last[:, 127:128], (1, 256))
    halo_send[4:5, :] = jnp.broadcast_to(last[:, 126:127], (1, 256))

    pl.semaphore_wait(bar, 11)
    halo_copy = remote(halo_send, halo_all.at[x], halo_s, halo_r.at[x], after)
    meta_copy = remote(meta_send, meta, meta_s, meta_r, twin)
    halo_copy.start()
    meta_copy.start()

    rows = lax.broadcasted_iota(jnp.int32, (128, 128), 0)
    lanes = lax.broadcasted_iota(jnp.int32, (128, 128), 1)
    eye = jnp.where(rows == lanes, 1.0, 0.0).astype(F32)

    def column(row):
        return jnp.sum(eye * row, axis=1, keepdims=True)

    lane8 = lax.broadcasted_iota(jnp.int32, (8, 128), 1)

    def conv_block(b):
        cur = jnp.broadcast_to(docs8[b + 1 : b + 2, :], (8, 128))
        prev = jnp.broadcast_to(docs8[b : b + 1, :], (8, 128))
        one = jnp.where(lane8 < 1, pltpu.roll(prev, 1, 1), pltpu.roll(cur, 1, 1))
        two = jnp.where(lane8 < 2, pltpu.roll(prev, 2, 1), pltpu.roll(cur, 2, 1))
        m1 = column(jnp.where(one == cur, 1.0, 0.0).astype(F32)[0:1, :])
        m2 = column(jnp.where(two == cur, 1.0, 0.0).astype(F32)[0:1, :])
        base = 8 + 128 * b
        i0 = inner[base : base + 128, :]
        i1 = inner[base - 1 : base + 127, :]
        i2 = inner[base - 2 : base + 126, :]
        value = t2 * i0 + t1 * (m1 * i1) + t0 * (m2 * i2)
        gate = go[128 * b : 128 * b + 128, :].astype(F32)
        conv_send[b] = (gate * value).astype(BF)
        if b == 0:
            fix_send[0:8, :] = value[0:8, :]
            fix_send[8:16, :] = gate[0:8, :]

    def tp_copy(b):
        slot = (b + 4 - x) % 4
        return remote(conv_send.at[b], conv_all.at[x], tp_send.at[slot], tp_recv.at[slot], (sp, b))

    def fix_copy(t):
        return remote(fix_send, fix_all.at[t], fix_s, fix_r.at[t], (sp, 0))

    for b in range(4):
        conv_block(b)

        @pl.when(x != b)
        def _():
            tp_copy(b).start()
            if b == 0:
                fix_copy(x).start()

        @pl.when(x == b)
        def _():
            conv_all[b] = conv_send[b]
            if b == 0:
                fix_all[0] = fix_send[...]

    meta_copy.wait_recv()

    def routing(table):
        e = [table[a : a + 1, :] for a in range(2)]
        ec = [column(v) for v in e]
        out_rows = []
        for a in range(2):
            same = ((ec[0] == e[a]) | (ec[1] == e[a])) & (rows < lanes)
            rank = jnp.sum(jnp.where(same, 1.0, 0.0).astype(F32), axis=0, keepdims=True)
            ei = e[a].astype(jnp.int32)

            unit = (ei & 3) + 4 * ((ei >> 3) & 3) + 16 * ((ei >> 5) & 3)
            out_rows.append((unit * 8 + rank.astype(jnp.int32), (ei >> 2) & 1))
        return out_rows

    slot_rows = lax.broadcasted_iota(jnp.int32, (512, 128), 0)
    slot_lanes = lax.broadcasted_iota(jnp.int32, (128, 512), 1).astype(F32)
    for s, table in ((0, meta_send), (1, meta)):
        source_core = c if s == 0 else 1 - c
        targets = []
        for slot, parity in routing(table):
            targets.append(jnp.where(parity == c, slot + 4 * source_core, -1))
        hit = (slot_rows == targets[0]) | (slot_rows == targets[1])
        pack[:, 128 * s : 128 * s + 128] = jnp.where(hit, 1.0, 0.0).astype(F32).astype(BF)
        weight = jnp.zeros((128, 512), F32)
        for a in range(2):
            tc = column(targets[a].astype(F32))
            wc = column(table[2 + a : 3 + a, :])
            weight = weight + jnp.where(slot_lanes == tc, wc, 0.0)
        high = weight.astype(BF)
        comb[0, 128 * s : 128 * s + 128, :] = high
        comb[1, 128 * s : 128 * s + 128, :] = (weight - high.astype(F32)).astype(BF)

    loads[3].wait()
    loads[4].wait()
    for j in range(1, 4):
        pltpu.make_async_remote_copy(
            src_ref=conv_send.at[0], dst_ref=conv_all.at[(x + 4 - j) % 4], send_sem=tp_send.at[j],
            recv_sem=tp_recv.at[j], device_id=tp_far[j], device_id_type=MESH,
        ).wait_recv()

    @pl.when(x == 0)
    def _():
        edge = lax.broadcasted_iota(jnp.int32, (8, 256), 0)
        first = docs[0:1, :].astype(F32)
        inside = jnp.where(sp == 0, 0.0, 1.0)
        for t in range(4):
            if t > 0:
                fix_copy(t).wait_recv()
            remote(halo_send, halo_all.at[t], halo_s, halo_r.at[t], after).wait_recv()
            from_behind = halo_all[t]
            m1 = jnp.where(from_behind[3:4] == first[:, 0:1], inside, 0.0)
            m2 = jnp.where(from_behind[4:5] == first[:, 0:1], inside, 0.0)
            m3 = jnp.where(from_behind[3:4] == first[:, 1:2], inside, 0.0)
            add0 = m1 * from_behind[0:1] + m2 * from_behind[1:2]
            add1 = m3 * from_behind[2:3]
            extra = jnp.where(edge == 0, add0, jnp.where(edge == 1, add1, 0.0))
            fixed = fix_all[t, 8:16, :] * (fix_all[t, 0:8, :] + extra)
            conv_all[t, 0:8, :] = fixed.astype(BF)

    total = jnp.zeros((128, 1), F32)
    for n in range(8):
        cols = slice(256 * n, 256 * n + 256)
        acc = jnp.zeros((128, 256), F32)
        for i in range(4):
            acc = acc + jnp.dot(conv_all[i], opv[256 * i : 256 * i + 256, cols], preferred_element_type=F32)
        value = res[:, cols].astype(F32) + acc.astype(BF).astype(F32)
        total = total + jnp.sum(value * value, axis=1, keepdims=True)
        carried[n] = value
    scale = lax.rsqrt(total / 2048.0 + 1e-6)

    def tok_copy(j):
        ks = pl.ds(2 * j, 2)
        return remote(tok.at[ks, pl.ds(0, 128)], tok.at[ks, pl.ds(128, 128)], tok_send.at[j], tok_recv.at[j], twin)

    for k in range(NCH):
        tok[k, 0:128, :] = (carried[k] * scale * gain[:, W * k : W * k + W]).astype(BF)
        if k % 2 == 1:
            tok_copy(k // 2).start()

    def plane(buf, p, k, axis, v):
        index = [slice(None)] * 3
        index[axis] = v
        return buf.at[(p, k, *index)]

    def move(buf, ss, rs, p, k, step):
        axis = (k + p) % 3
        return remote(
            plane(buf, p, k, axis, (here[axis] + step) % 4), plane(buf, p + 1, k, axis, here[axis]),
            ss.at[p, k, step - 1], rs.at[p, k, step - 1], along(axis, step),
        )

    def begin(buf, ss, rs, p, k):
        axis = (k + p) % 3
        for step in STEPS:
            move(buf, ss, rs, p, k, step).start()
        stay = plane(buf, p + 1, k, axis, here[axis])
        stay[...] = plane(buf, p, k, axis, here[axis])[...]

    def settle(buf, ss, rs, p, k):
        for step in STEPS:
            move(buf, ss, rs, p, k, step).wait_recv()

    def put(buf, k, value):
        buf[0, k] = value.reshape(CUBE).astype(BF)

    def rows_of(buf, k):
        return buf[3, k].astype(F32).reshape(512, W).astype(BF)

    for k in range(NCH):
        if k % 2 == 0:
            tok_copy(k // 2).wait_recv()
        put(there, k, jnp.dot(pack[...], tok[k], preferred_element_type=F32))
        begin(there, d_send, d_recv, 0, k)

    for p in range(1, 3):
        for k in range(NCH):
            settle(there, d_send, d_recv, p - 1, k)
            begin(there, d_send, d_recv, p, k)

    loads[5].wait()
    loads[6].wait()
    for k in range(NCH):
        settle(there, d_send, d_recv, 2, k)
        source = rows_of(there, k)
        rows_k = slice(W * k, W * k + W)
        for n in range(0, 1024, 512):
            g = jnp.dot(source, wg[rows_k, n : n + 512], preferred_element_type=F32)
            u = jnp.dot(source, wu[rows_k, n : n + 512], preferred_element_type=F32)
            if k == 0:
                gsum[:, n : n + 512] = g
                usum[:, n : n + 512] = u
            else:
                gsum[:, n : n + 512] += g
                usum[:, n : n + 512] += u

    @pl.loop(0, 16)
    def _(r):
        rs = pl.ds(pl.multiple_of(r * 32, 32), 32)
        g = gsum[rs, :]
        half = 0.5 * g
        hid[rs, :] = ((half + half * jnp.tanh(half)) * usum[rs, :]).astype(BF)

    loads[7].wait()
    for k in range(NCH):
        put(back, k, jnp.dot(hid[...], wd[:, W * k : W * k + W], preferred_element_type=F32))
        begin(back, c_send, c_recv, 0, k)

    for p in range(1, 3):
        for k in range(NCH):
            settle(back, c_send, c_recv, p - 1, k)
            begin(back, c_send, c_recv, p, k)

    def part_copy(k):
        return remote(part_send.at[k], part_recv.at[k], p_send.at[k], p_recv.at[k], twin)

    for k in range(NCH):
        settle(back, c_send, c_recv, 2, k)
        source = rows_of(back, k)
        both = jnp.dot(comb[0], source, preferred_element_type=F32) + jnp.dot(
            comb[1], source, preferred_element_type=F32
        )
        part_send[k] = both[128:]
        part_copy(k).start()
        carried[k] += both[:128]

    for k in range(NCH):
        part_copy(k).wait_recv()
        out[:, W * k : W * k + W] = (carried[k] + part_recv[k]).astype(BF)

    halo_copy.wait_send()
    meta_copy.wait_send()

    @pl.when(x != 0)
    def _():
        fix_copy(x).wait_send()

    for p in range(3):
        for k in range(NCH):
            for step in STEPS:
                move(there, d_send, d_recv, p, k, step).wait_send()
                move(back, c_send, c_recv, p, k, step).wait_send()
    for j in range(1, 4):
        pltpu.make_async_remote_copy(
            src_ref=conv_send.at[0], dst_ref=conv_all.at[0], send_sem=tp_send.at[j],
            recv_sem=tp_recv.at[j], device_id=tp_far[j], device_id_type=MESH,
        ).wait_send()
    for j in range(4):
        tok_copy(j).wait_send()
    for k in range(NCH):
        part_copy(k).wait_send()


def on_device(ci, gi, go, taps, docs, res, op, gain, ids, wts, wg, wu, wd):
    vmem = pl.BlockSpec(memory_space=pltpu.VMEM)
    hbm = pl.BlockSpec(memory_space=pl.ANY)
    dma = pltpu.SemaphoreType.DMA
    scratch = [
        pltpu.VMEM((512, 256), BF), pltpu.VMEM((512, 256), BF), pltpu.VMEM((512, 256), BF),
        pltpu.VMEM((128, 2048), BF), pltpu.VMEM((1024, 2048), BF),
        pltpu.VMEM((2048, 1024), BF), pltpu.VMEM((2048, 1024), BF), pltpu.VMEM((1024, 2048), BF),
        pltpu.VMEM((520, 256), F32), pltpu.VMEM((8, 256), F32), pltpu.VMEM((4, 8, 256), F32),
        pltpu.VMEM((16, 256), F32), pltpu.VMEM((4, 16, 256), F32),
        pltpu.VMEM((8, 128), jnp.int32), pltpu.VMEM((4, 128, 256), BF), pltpu.VMEM((4, 128, 256), BF),
        pltpu.VMEM((NCH, 128, W), F32), pltpu.VMEM((4, 128), F32), pltpu.VMEM((4, 128), F32),
        pltpu.VMEM((NCH, 256, W), BF), pltpu.VMEM((512, 256), BF), pltpu.VMEM((4, NCH, *CUBE), BF),
        pltpu.VMEM((512, 1024), F32), pltpu.VMEM((512, 1024), F32), pltpu.VMEM((512, 1024), BF),
        pltpu.VMEM((4, NCH, *CUBE), BF), pltpu.VMEM((2, 256, 512), BF),
        pltpu.VMEM((NCH, 128, W), F32), pltpu.VMEM((NCH, 128, W), F32),
        dma((8,)), dma, dma((4,)), dma, dma((4,)), dma, dma, dma((4,)), dma((4,)), dma((4,)), dma((4,)),
        dma((3, NCH, 3)), dma((3, NCH, 3)), dma((3, NCH, 3)), dma((3, NCH, 3)), dma((NCH,)), dma((NCH,)),
    ]
    return pl.pallas_call(
        layer_kernel,
        out_shape=jax.ShapeDtypeStruct((128, 2048), BF),
        in_specs=[hbm, hbm, hbm, vmem, vmem, hbm, hbm, vmem, vmem, vmem, hbm, hbm, hbm],
        out_specs=vmem,
        scratch_shapes=scratch,
        compiler_params=pltpu.CompilerParams(
            collective_id=0, has_side_effects=True, vmem_limit_bytes=64000000
        ),
    )(ci, gi, go, taps, docs.reshape(4, 128), res, op, gain.reshape(1, 2048), ids.T, wts.T, wg, wu, wd)


def solution(mesh):
    in_specs = (
        P("sp", "tp"),
        P("sp", "tp"),
        P("sp", "tp"),
        P(None, "tp"),
        P("sp"),
        P(("sp", "tp"), None),
        P(),
        P(),
        P(("sp", "tp"), None),
        P(("sp", "tp"), None),
        P(("sp", "tp"), None, None),
        P(("sp", "tp"), None, None),
        P(("sp", "tp"), None, None),
    )
    out_specs = P(("sp", "tp"), None)
    return jax.shard_map(
        on_device, mesh=mesh, in_specs=in_specs, out_specs=out_specs, check_vma=False
    )
```

time: 89.6 us -> 79.6 us (0.89)
  Pallas kernels: 87.4 us -> 77.5 us
    pallas_call x1, Pallas kernels: 87.4 us -> 77.5 us  [on_device(): pl.pallas_call(layer_kernel, out_shape=jax.ShapeDtypeStruct((128, 2048),...]
where the time goes in v2:
time: 79.6 us; the launch traced here: 79.4 us
  Pallas kernels  77.5 us (97%)
  local copies, waits for them, and re-layouts  1.88 us (2%)
    pallas_call x1, Pallas kernels, on_device(): pl.pallas_call(layer_kernel, out_shape=jax.ShapeDtypeStruct((128, 2048),...  77.5 us
    unnamed x1, local copies, waits for them, and re-layouts  1.88 us

profile of v2, /device:TPU:1, one launch (start us, length us, event | category | flops | bytes accessed | tf_op | source)
XLA Modules:
  0.0 79.4 jit_solution(16288067849755913489)
XLA Ops:
  0.0 77.5 %shard_map.127 = bf16[128,2048]{1,0:T(8,128)(2,1)} custom-call(bf16[512,256]{1,0:T(8,128)(2,1)} %ci_h.1, bf16[512,256]{1,0:T(8,128)(2,1)} %gi_h.1, bf16[512,256]{1,0:T(8,128)(2,1)} %go_h.1, bf16[3,256]{1,0:T(4,128)(2,1)} %taps.1, s32[4,128]{1,0:T(4,128)} %bitcast.5, bf16[128,2048]{1,0:T(8,128)(2,1)} %res_h.1, bf16[1024,2048]{1,0:T(8,128)(2,1)} %op_h.1, ...), custom_call_target="tpu_custom_call" | custom-call | tf_op jit(solution)/shard_map/pallas_call | solution.py:357
  77.5 1.9 %copy.15 = bf16[128,2048]{1,0:T(8,128)(2,1)} copy(bf16[128,2048]{1,0:T(8,128)(2,1)} %shard_map.127) | data formatting | bytes 1048576

commit v3 on v2

--- a/solution.py
+++ b/solution.py
@@ -8,16 +8,35 @@
 MESH = pl.DeviceIdType.MESH
 BF = jnp.bfloat16
 F32 = jnp.float32
-NCH = 8
-W = 256
-CUBE = (4, 4, 4, 8, W)
+NCH = 4
+W = 512
+PARTS = 1
+TOKS = 1
+PIECES = NCH * PARTS
+PW = W // PARTS
+CUBE = (2, 4, 4, 8, PW)
+HALF = 256
 STEPS = (2, 1, 3)
 
 
+def schedule():
+    ks, ts = range(NCH), range(PIECES)
+    order = []
+    for p in range(3):
+        for w in range(2):
+            order += [("D", w, k, p) for k in (ts if p else ks)]
+    order += [("F", 0, k) for k in ks] + [("S", 0)] + [("C", 0, k, 0) for k in ks]
+    order += [("F", 1, k) for k in ks] + [("S", 1)] + [("C", 1, k, 0) for k in ks]
+    for p in range(1, 3):
+        for w in range(2):
+            order += [("C", w, t, p) for t in ts]
+    return order + [("E", w, k) for w in range(2) for k in ks]
+
+
 def layer_kernel(
-    ci_h, gi_h, go_h, taps, docs, res_h, op_h, gain, ids, wts, wg_h, wu_h, wd_h,
+    ci_h, gi_h, go_h, taps_h, docs_h, res_h, op_h, gain_h, ids_h, wts_h, wg_h, wu_h, wd_h,
     out,
-    ci, gi, go, res, opv, wg, wu, wd,
+    ci, gi, go, taps, docs, ids, wts, gain, res, opv, wg, wu, wd,
     inner, halo_send, halo_all, fix_send, fix_all, docs8, conv_send, conv_all,
     carried, meta_send, meta, tok, pack, there, gsum, usum, hid, back, comb,
     part_send, part_recv,
@@ -43,9 +62,10 @@
     def load(src, dst, i):
         return pltpu.make_async_copy(src, dst, load_sem.at[i])
 
-    loads = [load(ci_h, ci, 0), load(gi_h, gi, 1), load(go_h, go, 2), load(res_h, res, 3),
-             load(op_h, opv, 4), load(wg_h.at[0], wg, 5), load(wu_h.at[0], wu, 6), load(wd_h.at[0], wd, 7)]
-    for i in range(3):
+    pairs = [(ci_h, ci), (gi_h, gi), (taps_h, taps), (docs_h, docs), (ids_h, ids), (wts_h, wts), (go_h, go),
+             (gain_h, gain), (res_h, res), (op_h, opv), (wg_h.at[0], wg), (wu_h.at[0], wu), (wd_h.at[0], wd)]
+    loads = [load(src, dst, i) for i, (src, dst) in enumerate(pairs)]
+    for i in range(7):
         loads[i].start()
 
     bar = pltpu.get_barrier_semaphore()
@@ -59,18 +79,16 @@
         for t in range(4):
             pl.semaphore_signal(bar, inc=1, device_id=((sp + 31) % 32, t), device_id_type=MESH)
 
+    for i in range(6):
+        loads[i].wait()
+    for i in range(7, 13):
+        loads[i].start()
     meta_send[0:2, :] = ids[...].astype(F32)
     meta_send[2:4, :] = wts[...]
     docs8[0:1, :] = jnp.full((1, 128), -1, jnp.int32)
     docs8[1:5, :] = docs[...]
     inner[0:8, :] = jnp.zeros((8, 256), F32)
-
-    for i in range(2):
-        loads[i].wait()
     inner[8:520, :] = ci[...].astype(F32) * gi[...].astype(F32)
-    loads[2].wait()
-    for i in range(3, 8):
-        loads[i].start()
 
     def remote(src, dst, ssem, rsem, dev):
         return pltpu.make_async_remote_copy(
@@ -127,6 +145,7 @@
     def fix_copy(t):
         return remote(fix_send, fix_all.at[t], fix_s, fix_r.at[t], (sp, 0))
 
+    loads[6].wait()
     for b in range(4):
         conv_block(b)
 
@@ -153,7 +172,8 @@
             rank = jnp.sum(jnp.where(same, 1.0, 0.0).astype(F32), axis=0, keepdims=True)
             ei = e[a].astype(jnp.int32)
 
-            unit = (ei & 3) + 4 * ((ei >> 3) & 3) + 16 * ((ei >> 5) & 3)
+            ahead = (((ei >> 5) & 3) - z + 4) & 3
+            unit = (ei & 3) + 4 * ((ei >> 3) & 3) + 16 * (2 * (ahead & 1) + (ahead >> 1))
             out_rows.append((unit * 8 + rank.astype(jnp.int32), (ei >> 2) & 1))
         return out_rows
 
@@ -175,8 +195,8 @@
         comb[0, 128 * s : 128 * s + 128, :] = high
         comb[1, 128 * s : 128 * s + 128, :] = (weight - high.astype(F32)).astype(BF)
 
-    loads[3].wait()
-    loads[4].wait()
+    for i in (7, 8, 9):
+        loads[i].wait()
     for j in range(1, 4):
         pltpu.make_async_remote_copy(
             src_ref=conv_send.at[0], dst_ref=conv_all.at[(x + 4 - j) % 4], send_sem=tp_send.at[j],
@@ -203,9 +223,9 @@
             conv_all[t, 0:8, :] = fixed.astype(BF)
 
     total = jnp.zeros((128, 1), F32)
-    for n in range(8):
-        cols = slice(256 * n, 256 * n + 256)
-        acc = jnp.zeros((128, 256), F32)
+    for n in range(NCH):
+        cols = slice(W * n, W * n + W)
+        acc = jnp.zeros((128, W), F32)
         for i in range(4):
             acc = acc + jnp.dot(conv_all[i], opv[256 * i : 256 * i + 256, cols], preferred_element_type=F32)
         value = res[:, cols].astype(F32) + acc.astype(BF).astype(F32)
@@ -214,99 +234,137 @@
     scale = lax.rsqrt(total / 2048.0 + 1e-6)
 
     def tok_copy(j):
-        ks = pl.ds(2 * j, 2)
+        ks = pl.ds(TOKS * j, TOKS)
         return remote(tok.at[ks, pl.ds(0, 128)], tok.at[ks, pl.ds(128, 128)], tok_send.at[j], tok_recv.at[j], twin)
 
     for k in range(NCH):
         tok[k, 0:128, :] = (carried[k] * scale * gain[:, W * k : W * k + W]).astype(BF)
-        if k % 2 == 1:
-            tok_copy(k // 2).start()
-
-    def plane(buf, p, k, axis, v):
+        if (k + 1) % TOKS == 0:
+            tok_copy(k // TOKS).start()
+
+    def plane(buf, w, p, k, axis, v):
         index = [slice(None)] * 3
         index[axis] = v
-        return buf.at[(p, k, *index)]
-
-    def move(buf, ss, rs, p, k, step):
-        axis = (k + p) % 3
-        return remote(
-            plane(buf, p, k, axis, (here[axis] + step) % 4), plane(buf, p + 1, k, axis, here[axis]),
-            ss.at[p, k, step - 1], rs.at[p, k, step - 1], along(axis, step),
-        )
-
-    def begin(buf, ss, rs, p, k):
-        axis = (k + p) % 3
-        for step in STEPS:
-            move(buf, ss, rs, p, k, step).start()
-        stay = plane(buf, p + 1, k, axis, here[axis])
-        stay[...] = plane(buf, p, k, axis, here[axis])[...]
-
-    def settle(buf, ss, rs, p, k):
-        for step in STEPS:
-            move(buf, ss, rs, p, k, step).wait_recv()
-
-    def put(buf, k, value):
-        buf[0, k] = value.reshape(CUBE).astype(BF)
-
-    def rows_of(buf, k):
-        return buf[3, k].astype(F32).reshape(512, W).astype(BF)
-
-    for k in range(NCH):
-        if k % 2 == 0:
-            tok_copy(k // 2).wait_recv()
-        put(there, k, jnp.dot(pack[...], tok[k], preferred_element_type=F32))
-        begin(there, d_send, d_recv, 0, k)
-
-    for p in range(1, 3):
-        for k in range(NCH):
-            settle(there, d_send, d_recv, p - 1, k)
-            begin(there, d_send, d_recv, p, k)
-
-    loads[5].wait()
-    loads[6].wait()
-    for k in range(NCH):
-        settle(there, d_send, d_recv, 2, k)
-        source = rows_of(there, k)
+        return buf.at[(w, p, k, *index)]
+
+    def axis_of(w, p, k):
+        return (k + p + w) % 3
+
+    def moves(buf, ss, rs, w, p, k, sign):
+        axis = axis_of(w, p, k)
+        found = []
+        if axis == 0:
+            for j in range(2):
+                step = (w + 2 * j) * sign % 4
+                if step != 0:
+                    found.append((plane(buf, w, p, k, 0, j), plane(buf, w, p + 1, k, 0, j), step))
+        else:
+            for step in STEPS:
+                source = plane(buf, w, p, k, axis, (here[axis] + step) % 4)
+                found.append((source, plane(buf, w, p + 1, k, axis, here[axis]), step))
+        return [
+            remote(src, dst, ss.at[w, p, k, n], rs.at[w, p, k, n], along(axis, step))
+            for n, (src, dst, step) in enumerate(found)
+        ]
+
+    def begin(buf, ss, rs, w, p, k, sign):
+        for copy in moves(buf, ss, rs, w, p, k, sign):
+            copy.start()
+        axis = axis_of(w, p, k)
+        if axis != 0:
+            stay = plane(buf, w, p + 1, k, axis, here[axis])
+            stay[...] = plane(buf, w, p, k, axis, here[axis])[...]
+        elif w == 0:
+            stay = plane(buf, w, p + 1, k, 0, 0)
+            stay[...] = plane(buf, w, p, k, 0, 0)[...]
+
+    def settle(buf, ss, rs, w, p, k, sign):
+        for copy in moves(buf, ss, rs, w, p, k, sign):
+            copy.wait_recv()
+
+    out_way = (there, d_send, d_recv)
+    home_way = (back, c_send, c_recv)
+
+    def pieces(k):
+        return range(PARTS * k, PARTS * k + PARTS)
+
+    def put(buf, w, k, value):
+        for i, t in enumerate(pieces(k)):
+            buf[w, 0, t] = value[:, PW * i : PW * i + PW].reshape(CUBE).astype(BF)
+
+    def rows_of(buf, w, k):
+        parts = [buf[w, 3, t].astype(F32).reshape(HALF, PW).astype(BF) for t in pieces(k)]
+        return jnp.concatenate(parts, axis=1)
+
+    def step_out(w, k, p):
+        if p == 0:
+            if w == 0 and k % TOKS == 0:
+                tok_copy(k // TOKS).wait_recv()
+            packed = jnp.dot(pack[HALF * w : HALF * w + HALF, :], tok[k], preferred_element_type=F32)
+            put(there, w, k, packed)
+            for t in pieces(k):
+                begin(*out_way, w, p, t, 1)
+        else:
+            settle(*out_way, w, p - 1, k, 1)
+            begin(*out_way, w, p, k, 1)
+
+    def gate_up(w, k):
+        if w == 0 and k == 0:
+            loads[10].wait()
+            loads[11].wait()
+        for t in pieces(k):
+            settle(*out_way, w, 2, t, 1)
+        source = rows_of(there, w, k)
         rows_k = slice(W * k, W * k + W)
-        for n in range(0, 1024, 512):
-            g = jnp.dot(source, wg[rows_k, n : n + 512], preferred_element_type=F32)
-            u = jnp.dot(source, wu[rows_k, n : n + 512], preferred_element_type=F32)
-            if k == 0:
-                gsum[:, n : n + 512] = g
-                usum[:, n : n + 512] = u
-            else:
-                gsum[:, n : n + 512] += g
-                usum[:, n : n + 512] += u
-
-    @pl.loop(0, 16)
-    def _(r):
-        rs = pl.ds(pl.multiple_of(r * 32, 32), 32)
-        g = gsum[rs, :]
-        half = 0.5 * g
-        hid[rs, :] = ((half + half * jnp.tanh(half)) * usum[rs, :]).astype(BF)
-
-    loads[7].wait()
-    for k in range(NCH):
-        put(back, k, jnp.dot(hid[...], wd[:, W * k : W * k + W], preferred_element_type=F32))
-        begin(back, c_send, c_recv, 0, k)
-
-    for p in range(1, 3):
-        for k in range(NCH):
-            settle(back, c_send, c_recv, p - 1, k)
-            begin(back, c_send, c_recv, p, k)
+        g = jnp.dot(source, wg[rows_k, :], preferred_element_type=F32)
+        u = jnp.dot(source, wu[rows_k, :], preferred_element_type=F32)
+        if k == 0:
+            gsum[w] = g
+            usum[w] = u
+        else:
+            gsum[w] += g
+            usum[w] += u
+
+    def activate(w):
+        @pl.loop(0, 8)
+        def _(r):
+            rs = pl.ds(pl.multiple_of(r * 32, 32), 32)
+            half = 0.5 * gsum[w, rs, :]
+            hid[w, rs, :] = ((half + half * jnp.tanh(half)) * usum[w, rs, :]).astype(BF)
+
+        if w == 0:
+            loads[12].wait()
+
+    def step_home(w, k, p):
+        if p == 0:
+            put(back, w, k, jnp.dot(hid[w], wd[:, W * k : W * k + W], preferred_element_type=F32))
+            for t in pieces(k):
+                begin(*home_way, w, p, t, -1)
+        else:
+            settle(*home_way, w, p - 1, k, -1)
+            begin(*home_way, w, p, k, -1)
 
     def part_copy(k):
         return remote(part_send.at[k], part_recv.at[k], p_send.at[k], p_recv.at[k], twin)
 
-    for k in range(NCH):
-        settle(back, c_send, c_recv, 2, k)
-        source = rows_of(back, k)
-        both = jnp.dot(comb[0], source, preferred_element_type=F32) + jnp.dot(
-            comb[1], source, preferred_element_type=F32
+    def collect(w, k):
+        for t in pieces(k):
+            settle(*home_way, w, 2, t, -1)
+        source = rows_of(back, w, k)
+        slots = slice(HALF * w, HALF * w + HALF)
+        both = jnp.dot(comb[0, :, slots], source, preferred_element_type=F32) + jnp.dot(
+            comb[1, :, slots], source, preferred_element_type=F32
         )
-        part_send[k] = both[128:]
-        part_copy(k).start()
         carried[k] += both[:128]
+        if w == 0:
+            part_send[k] = both[128:]
+        else:
+            part_send[k] += both[128:]
+            part_copy(k).start()
+
+    actions = {"D": step_out, "F": gate_up, "S": activate, "C": step_home, "E": collect}
+    for name, *where in schedule():
+        actions[name](*where)
 
     for k in range(NCH):
         part_copy(k).wait_recv()
@@ -319,17 +377,17 @@
     def _():
         fix_copy(x).wait_send()
 
-    for p in range(3):
-        for k in range(NCH):
-            for step in STEPS:
-                move(there, d_send, d_recv, p, k, step).wait_send()
-                move(back, c_send, c_recv, p, k, step).wait_send()
+    for w in range(2):
+        for p in range(3):
+            for k in range(PIECES):
+                for copy in moves(*out_way, w, p, k, 1) + moves(*home_way, w, p, k, -1):
+                    copy.wait_send()
     for j in range(1, 4):
         pltpu.make_async_remote_copy(
             src_ref=conv_send.at[0], dst_ref=conv_all.at[0], send_sem=tp_send.at[j],
             recv_sem=tp_recv.at[j], device_id=tp_far[j], device_id_type=MESH,
         ).wait_send()
-    for j in range(4):
+    for j in range(NCH // TOKS):
         tok_copy(j).wait_send()
     for k in range(NCH):
         part_copy(k).wait_send()
@@ -337,33 +395,37 @@
 
 def on_device(ci, gi, go, taps, docs, res, op, gain, ids, wts, wg, wu, wd):
     vmem = pl.BlockSpec(memory_space=pltpu.VMEM)
-    hbm = pl.BlockSpec(memory_space=pl.ANY)
+    hbm = pl.BlockSpec(memory_space=pltpu.HBM)
     dma = pltpu.SemaphoreType.DMA
     scratch = [
         pltpu.VMEM((512, 256), BF), pltpu.VMEM((512, 256), BF), pltpu.VMEM((512, 256), BF),
+        pltpu.VMEM((3, 256), BF), pltpu.VMEM((4, 128), jnp.int32), pltpu.VMEM((2, 128), jnp.int32),
+        pltpu.VMEM((2, 128), F32), pltpu.VMEM((1, 2048), F32),
         pltpu.VMEM((128, 2048), BF), pltpu.VMEM((1024, 2048), BF),
         pltpu.VMEM((2048, 1024), BF), pltpu.VMEM((2048, 1024), BF), pltpu.VMEM((1024, 2048), BF),
         pltpu.VMEM((520, 256), F32), pltpu.VMEM((8, 256), F32), pltpu.VMEM((4, 8, 256), F32),
         pltpu.VMEM((16, 256), F32), pltpu.VMEM((4, 16, 256), F32),
         pltpu.VMEM((8, 128), jnp.int32), pltpu.VMEM((4, 128, 256), BF), pltpu.VMEM((4, 128, 256), BF),
         pltpu.VMEM((NCH, 128, W), F32), pltpu.VMEM((4, 128), F32), pltpu.VMEM((4, 128), F32),
-        pltpu.VMEM((NCH, 256, W), BF), pltpu.VMEM((512, 256), BF), pltpu.VMEM((4, NCH, *CUBE), BF),
-        pltpu.VMEM((512, 1024), F32), pltpu.VMEM((512, 1024), F32), pltpu.VMEM((512, 1024), BF),
-        pltpu.VMEM((4, NCH, *CUBE), BF), pltpu.VMEM((2, 256, 512), BF),
+        pltpu.VMEM((NCH, 256, W), BF), pltpu.VMEM((512, 256), BF), pltpu.VMEM((2, 4, PIECES, *CUBE), BF),
+        pltpu.VMEM((2, HALF, 1024), F32), pltpu.VMEM((2, HALF, 1024), F32), pltpu.VMEM((2, HALF, 1024), BF),
+        pltpu.VMEM((2, 4, PIECES, *CUBE), BF), pltpu.VMEM((2, 256, 512), BF),
         pltpu.VMEM((NCH, 128, W), F32), pltpu.VMEM((NCH, 128, W), F32),
-        dma((8,)), dma, dma((4,)), dma, dma((4,)), dma, dma, dma((4,)), dma((4,)), dma((4,)), dma((4,)),
-        dma((3, NCH, 3)), dma((3, NCH, 3)), dma((3, NCH, 3)), dma((3, NCH, 3)), dma((NCH,)), dma((NCH,)),
+        dma((13,)), dma, dma((4,)), dma, dma((4,)), dma, dma, dma((4,)), dma((4,)), dma((NCH,)), dma((NCH,)),
+        dma((2, 3, PIECES, 3)), dma((2, 3, PIECES, 3)), dma((2, 3, PIECES, 3)), dma((2, 3, PIECES, 3)), dma((NCH,)), dma((NCH,)),
     ]
+    arrays = (ci, gi, go, taps, docs.reshape(4, 128), res, op, gain.reshape(1, 2048), ids.T, wts.T, wg, wu, wd)
+    arrays = [pltpu.with_memory_space_constraint(v, pltpu.HBM) for v in arrays]
     return pl.pallas_call(
         layer_kernel,
         out_shape=jax.ShapeDtypeStruct((128, 2048), BF),
-        in_specs=[hbm, hbm, hbm, vmem, vmem, hbm, hbm, vmem, vmem, vmem, hbm, hbm, hbm],
+        in_specs=[hbm] * 13,
         out_specs=vmem,
         scratch_shapes=scratch,
         compiler_params=pltpu.CompilerParams(
-            collective_id=0, has_side_effects=True, vmem_limit_bytes=64000000
+            collective_id=0, has_side_effects=True, vmem_limit_bytes=54000000
         ),
-    )(ci, gi, go, taps, docs.reshape(4, 128), res, op, gain.reshape(1, 2048), ids.T, wts.T, wg, wu, wd)
+    )(*arrays)
 
 
 def solution(mesh):

time: 79.6 us -> 73.9 us (0.928)
  Pallas kernels: 77.5 us -> 73 us
  local copies, waits for them, and re-layouts: 1.88 us -> 0.8 us
    pallas_call x1, Pallas kernels: 77.5 us -> 73 us  [on_device(): pl.pallas_call(layer_kernel, out_shape=jax.ShapeDtypeStruct((128, 2048),...]
    unnamed x1, local copies, waits for them, and re-layouts: 1.88 us -> 0.8 us
where the time goes in v3:
time: 73.9 us; the launch traced here: 73.8 us
  Pallas kernels  73 us (99%)
  local copies, waits for them, and re-layouts  0.8 us (1%)
    pallas_call x1, Pallas kernels, on_device(): pl.pallas_call(layer_kernel, out_shape=jax.ShapeDtypeStruct((128, 2048),...  73 us

profile of v3, /device:TPU:1, one launch (start us, length us, event | category | flops | bytes accessed | tf_op | source)
XLA Modules:
  0.0 73.8 jit_solution(2122987425396227248)
XLA Ops:
  0.0 73.0 %shard_map.127 = bf16[128,2048]{1,0:T(8,128)(2,1)S(1)} custom-call(bf16[512,256]{1,0:T(8,128)(2,1)} %ci_h.1, bf16[512,256]{1,0:T(8,128)(2,1)} %gi_h.1, bf16[512,256]{1,0:T(8,128)(2,1)} %go_h.1, bf16[3,256]{1,0:T(4,128)(2,1)} %taps_h.1, s32[4,128]{1,0:T(4,128)} %bitcast.5, bf16[128,2048]{1,0:T(8,128)(2,1)} %res_h.1, bf16[1024,2048]{1,0:T(8,128)(2,1)} %op_h.1, ...), custom_call_target="tpu_custom_call" | custom-call | tf_op jit(solution)/shard_map/pallas_call | solution.py:419
  73.0 0.8 %copy.15 = bf16[128,2048]{1,0:T(8,128)(2,1)} copy(bf16[128,2048]{1,0:T(8,128)(2,1)S(1)} %shard_map.127) | data formatting | bytes 1048576

commit v4 on v3

--- a/solution.py
+++ b/solution.py
@@ -8,28 +8,26 @@
 MESH = pl.DeviceIdType.MESH
 BF = jnp.bfloat16
 F32 = jnp.float32
-NCH = 4
-W = 512
-PARTS = 1
-TOKS = 1
-PIECES = NCH * PARTS
-PW = W // PARTS
-CUBE = (2, 4, 4, 8, PW)
+WIDTHS = (512, 512, 512, 512)
+STARTS = (0, 512, 1024, 1536)
+NCH = len(WIDTHS)
+WIDE = max(WIDTHS)
+CUBE = (2, 4, 4, 8, WIDE)
 HALF = 256
-STEPS = (2, 1, 3)
+STEPS = (1, 3, 2)
 
 
 def schedule():
-    ks, ts = range(NCH), range(PIECES)
+    ks = range(NCH)
     order = []
     for p in range(3):
         for w in range(2):
-            order += [("D", w, k, p) for k in (ts if p else ks)]
-    order += [("F", 0, k) for k in ks] + [("S", 0)] + [("C", 0, k, 0) for k in ks]
-    order += [("F", 1, k) for k in ks] + [("S", 1)] + [("C", 1, k, 0) for k in ks]
+            order += [("D", w, k, p) for k in ks]
+    order += [("F", 0, k) for k in ks] + [("C", 0, k, 0) for k in ks]
+    order += [("F", 1, k) for k in ks] + [("C", 1, k, 0) for k in ks]
     for p in range(1, 3):
         for w in range(2):
-            order += [("C", w, t, p) for t in ts]
+            order += [("C", w, k, p) for k in ks]
     return order + [("E", w, k) for w in range(2) for k in ks]
 
 
@@ -48,12 +46,13 @@
     c = sp % 2
     y = (sp // 2) % 4
     z = sp // 8
-    here = [z, y, x]
+    here = [z, y + c * (x - y), x + c * (y - x)]
 
     def along(axis, step):
-        at = [z, y, x]
+        at = list(here)
         at[axis] = (at[axis] + step) % 4
-        return ((at[0] * 4 + at[1]) * 2 + c, at[2])
+        row, col = at[1] + c * (at[2] - at[1]), at[2] + c * (at[1] - at[2])
+        return ((at[0] * 4 + row) * 2 + c, col)
 
     twin = (sp + 1 - 2 * c, x)
     after = ((sp + 1) % 32, 0)
@@ -138,9 +137,8 @@
             fix_send[0:8, :] = value[0:8, :]
             fix_send[8:16, :] = gate[0:8, :]
 
-    def tp_copy(b):
-        slot = (b + 4 - x) % 4
-        return remote(conv_send.at[b], conv_all.at[x], tp_send.at[slot], tp_recv.at[slot], (sp, b))
+    def tp_copy(j):
+        return remote(conv_send.at[(x + j) % 4], conv_all.at[x], tp_send.at[j], tp_recv.at[j], tp_far[j])
 
     def fix_copy(t):
         return remote(fix_send, fix_all.at[t], fix_s, fix_r.at[t], (sp, 0))
@@ -149,17 +147,17 @@
     for b in range(4):
         conv_block(b)
 
-        @pl.when(x != b)
-        def _():
-            tp_copy(b).start()
-            if b == 0:
-                fix_copy(x).start()
-
-        @pl.when(x == b)
-        def _():
-            conv_all[b] = conv_send[b]
-            if b == 0:
-                fix_all[0] = fix_send[...]
+    @pl.when(x != 0)
+    def _():
+        fix_copy(x).start()
+
+    for j in STEPS:
+        tp_copy(j).start()
+    conv_all[x] = conv_send[x]
+
+    @pl.when(x == 0)
+    def _():
+        fix_all[0] = fix_send[...]
 
     meta_copy.wait_recv()
 
@@ -173,7 +171,8 @@
             ei = e[a].astype(jnp.int32)
 
             ahead = (((ei >> 5) & 3) - z + 4) & 3
-            unit = (ei & 3) + 4 * ((ei >> 3) & 3) + 16 * (2 * (ahead & 1) + (ahead >> 1))
+            row, col = (ei >> 3) & 3, ei & 3
+            unit = col + c * (row - col) + 4 * (row + c * (col - row)) + 16 * (2 * (ahead & 1) + (ahead >> 1))
             out_rows.append((unit * 8 + rank.astype(jnp.int32), (ei >> 2) & 1))
         return out_rows
 
@@ -223,32 +222,37 @@
             conv_all[t, 0:8, :] = fixed.astype(BF)
 
     total = jnp.zeros((128, 1), F32)
-    for n in range(NCH):
-        cols = slice(W * n, W * n + W)
-        acc = jnp.zeros((128, W), F32)
-        for i in range(4):
-            acc = acc + jnp.dot(conv_all[i], opv[256 * i : 256 * i + 256, cols], preferred_element_type=F32)
-        value = res[:, cols].astype(F32) + acc.astype(BF).astype(F32)
-        total = total + jnp.sum(value * value, axis=1, keepdims=True)
-        carried[n] = value
+    for k in range(NCH):
+        for n in range(0, WIDTHS[k], 256):
+            cols = slice(STARTS[k] + n, STARTS[k] + n + 256)
+            acc = jnp.zeros((128, 256), F32)
+            for i in range(4):
+                acc = acc + jnp.dot(conv_all[i], opv[256 * i : 256 * i + 256, cols], preferred_element_type=F32)
+            value = res[:, cols].astype(F32) + acc.astype(BF).astype(F32)
+            total = total + jnp.sum(value * value, axis=1, keepdims=True)
+            carried[k, :, n : n + 256] = value
     scale = lax.rsqrt(total / 2048.0 + 1e-6)
 
-    def tok_copy(j):
-        ks = pl.ds(TOKS * j, TOKS)
-        return remote(tok.at[ks, pl.ds(0, 128)], tok.at[ks, pl.ds(128, 128)], tok_send.at[j], tok_recv.at[j], twin)
+    def tok_copy(k):
+        lanes_k = pl.ds(0, WIDTHS[k])
+        return remote(
+            tok.at[k, pl.ds(0, 128), lanes_k], tok.at[k, pl.ds(128, 128), lanes_k],
+            tok_send.at[k], tok_recv.at[k], twin,
+        )
 
     for k in range(NCH):
-        tok[k, 0:128, :] = (carried[k] * scale * gain[:, W * k : W * k + W]).astype(BF)
-        if (k + 1) % TOKS == 0:
-            tok_copy(k // TOKS).start()
+        width, start = WIDTHS[k], STARTS[k]
+        normed = carried[k, :, :width] * scale * gain[:, start : start + width]
+        tok[k, 0:128, :width] = normed.astype(BF)
+        tok_copy(k).start()
 
     def plane(buf, w, p, k, axis, v):
         index = [slice(None)] * 3
         index[axis] = v
-        return buf.at[(w, p, k, *index)]
+        return buf.at[(w, p, k, *index, slice(None), pl.ds(0, WIDTHS[k]))]
 
     def axis_of(w, p, k):
-        return (k + p + w) % 3
+        return (k + 2 * p + w) % 3
 
     def moves(buf, ss, rs, w, p, k, sign):
         axis = axis_of(w, p, k)
@@ -285,37 +289,40 @@
     out_way = (there, d_send, d_recv)
     home_way = (back, c_send, c_recv)
 
-    def pieces(k):
-        return range(PARTS * k, PARTS * k + PARTS)
+    def columns(k):
+        return slice(STARTS[k], STARTS[k] + WIDTHS[k])
 
     def put(buf, w, k, value):
-        for i, t in enumerate(pieces(k)):
-            buf[w, 0, t] = value[:, PW * i : PW * i + PW].reshape(CUBE).astype(BF)
+        buf[w, 0, k, :, :, :, :, : WIDTHS[k]] = value.reshape(*CUBE[:4], WIDTHS[k]).astype(BF)
 
     def rows_of(buf, w, k):
-        parts = [buf[w, 3, t].astype(F32).reshape(HALF, PW).astype(BF) for t in pieces(k)]
-        return jnp.concatenate(parts, axis=1)
+        return buf[w, 3, k, :, :, :, :, : WIDTHS[k]].astype(F32).reshape(HALF, WIDTHS[k]).astype(BF)
 
     def step_out(w, k, p):
         if p == 0:
-            if w == 0 and k % TOKS == 0:
-                tok_copy(k // TOKS).wait_recv()
-            packed = jnp.dot(pack[HALF * w : HALF * w + HALF, :], tok[k], preferred_element_type=F32)
-            put(there, w, k, packed)
-            for t in pieces(k):
-                begin(*out_way, w, p, t, 1)
+            if w == 0:
+                tok_copy(k).wait_recv()
+            source = tok[k, :, : WIDTHS[k]]
+            put(there, w, k, jnp.dot(pack[HALF * w : HALF * w + HALF, :], source, preferred_element_type=F32))
         else:
             settle(*out_way, w, p - 1, k, 1)
-            begin(*out_way, w, p, k, 1)
+        begin(*out_way, w, p, k, 1)
 
     def gate_up(w, k):
         if w == 0 and k == 0:
             loads[10].wait()
             loads[11].wait()
-        for t in pieces(k):
-            settle(*out_way, w, 2, t, 1)
+        settle(*out_way, w, 2, k, 1)
         source = rows_of(there, w, k)
-        rows_k = slice(W * k, W * k + W)
+        rows_k = columns(k)
+        if k == NCH - 1:
+            for n in range(0, 1024, 256):
+                block = slice(n, n + 256)
+                g = gsum[w, :, block] + jnp.dot(source, wg[rows_k, block], preferred_element_type=F32)
+                u = usum[w, :, block] + jnp.dot(source, wu[rows_k, block], preferred_element_type=F32)
+                half = 0.5 * g
+                hid[w, :, block] = ((half + half * jnp.tanh(half)) * u).astype(BF)
+            return
         g = jnp.dot(source, wg[rows_k, :], preferred_element_type=F32)
         u = jnp.dot(source, wu[rows_k, :], preferred_element_type=F32)
         if k == 0:
@@ -325,50 +332,41 @@
             gsum[w] += g
             usum[w] += u
 
-    def activate(w):
-        @pl.loop(0, 8)
-        def _(r):
-            rs = pl.ds(pl.multiple_of(r * 32, 32), 32)
-            half = 0.5 * gsum[w, rs, :]
-            hid[w, rs, :] = ((half + half * jnp.tanh(half)) * usum[w, rs, :]).astype(BF)
-
-        if w == 0:
+    def step_home(w, k, p):
+        if w == 0 and k == 0 and p == 0:
             loads[12].wait()
-
-    def step_home(w, k, p):
         if p == 0:
-            put(back, w, k, jnp.dot(hid[w], wd[:, W * k : W * k + W], preferred_element_type=F32))
-            for t in pieces(k):
-                begin(*home_way, w, p, t, -1)
+            put(back, w, k, jnp.dot(hid[w], wd[:, columns(k)], preferred_element_type=F32))
         else:
             settle(*home_way, w, p - 1, k, -1)
-            begin(*home_way, w, p, k, -1)
+        begin(*home_way, w, p, k, -1)
 
     def part_copy(k):
-        return remote(part_send.at[k], part_recv.at[k], p_send.at[k], p_recv.at[k], twin)
+        part = (k, slice(None), pl.ds(0, WIDTHS[k]))
+        return remote(part_send.at[part], part_recv.at[part], p_send.at[k], p_recv.at[k], twin)
 
     def collect(w, k):
-        for t in pieces(k):
-            settle(*home_way, w, 2, t, -1)
+        settle(*home_way, w, 2, k, -1)
         source = rows_of(back, w, k)
         slots = slice(HALF * w, HALF * w + HALF)
         both = jnp.dot(comb[0, :, slots], source, preferred_element_type=F32) + jnp.dot(
             comb[1, :, slots], source, preferred_element_type=F32
         )
-        carried[k] += both[:128]
+        carried[k, :, : WIDTHS[k]] += both[:128]
         if w == 0:
-            part_send[k] = both[128:]
+            part_send[k, :, : WIDTHS[k]] = both[128:]
         else:
-            part_send[k] += both[128:]
+            part_send[k, :, : WIDTHS[k]] += both[128:]
             part_copy(k).start()
 
-    actions = {"D": step_out, "F": gate_up, "S": activate, "C": step_home, "E": collect}
+    actions = {"D": step_out, "F": gate_up, "C": step_home, "E": collect}
     for name, *where in schedule():
         actions[name](*where)
 
     for k in range(NCH):
         part_copy(k).wait_recv()
-        out[:, W * k : W * k + W] = (carried[k] + part_recv[k]).astype(BF)
+        width = WIDTHS[k]
+        out[:, columns(k)] = (carried[k, :, :width] + part_recv[k, :, :width]).astype(BF)
 
     halo_copy.wait_send()
     meta_copy.wait_send()
@@ -379,7 +377,7 @@
 
     for w in range(2):
         for p in range(3):
-            for k in range(PIECES):
+            for k in range(NCH):
                 for copy in moves(*out_way, w, p, k, 1) + moves(*home_way, w, p, k, -1):
                     copy.wait_send()
     for j in range(1, 4):
@@ -387,7 +385,7 @@
             src_ref=conv_send.at[0], dst_ref=conv_all.at[0], send_sem=tp_send.at[j],
             recv_sem=tp_recv.at[j], device_id=tp_far[j], device_id_type=MESH,
         ).wait_send()
-    for j in range(NCH // TOKS):
+    for j in range(NCH):
         tok_copy(j).wait_send()
     for k in range(NCH):
         part_copy(k).wait_send()
@@ -406,13 +404,13 @@
         pltpu.VMEM((520, 256), F32), pltpu.VMEM((8, 256), F32), pltpu.VMEM((4, 8, 256), F32),
         pltpu.VMEM((16, 256), F32), pltpu.VMEM((4, 16, 256), F32),
         pltpu.VMEM((8, 128), jnp.int32), pltpu.VMEM((4, 128, 256), BF), pltpu.VMEM((4, 128, 256), BF),
-        pltpu.VMEM((NCH, 128, W), F32), pltpu.VMEM((4, 128), F32), pltpu.VMEM((4, 128), F32),
-        pltpu.VMEM((NCH, 256, W), BF), pltpu.VMEM((512, 256), BF), pltpu.VMEM((2, 4, PIECES, *CUBE), BF),
+        pltpu.VMEM((NCH, 128, WIDE), F32), pltpu.VMEM((4, 128), F32), pltpu.VMEM((4, 128), F32),
+        pltpu.VMEM((NCH, 256, WIDE), BF), pltpu.VMEM((512, 256), BF), pltpu.VMEM((2, 4, NCH, *CUBE), BF),
         pltpu.VMEM((2, HALF, 1024), F32), pltpu.VMEM((2, HALF, 1024), F32), pltpu.VMEM((2, HALF, 1024), BF),
-        pltpu.VMEM((2, 4, PIECES, *CUBE), BF), pltpu.VMEM((2, 256, 512), BF),
-        pltpu.VMEM((NCH, 128, W), F32), pltpu.VMEM((NCH, 128, W), F32),
+        pltpu.VMEM((2, 4, NCH, *CUBE), BF), pltpu.VMEM((2, 256, 512), BF),
+        pltpu.VMEM((NCH, 128, WIDE), F32), pltpu.VMEM((NCH, 128, WIDE), F32),
         dma((13,)), dma, dma((4,)), dma, dma((4,)), dma, dma, dma((4,)), dma((4,)), dma((NCH,)), dma((NCH,)),
-        dma((2, 3, PIECES, 3)), dma((2, 3, PIECES, 3)), dma((2, 3, PIECES, 3)), dma((2, 3, PIECES, 3)), dma((NCH,)), dma((NCH,)),
+        dma((2, 3, NCH, 3)), dma((2, 3, NCH, 3)), dma((2, 3, NCH, 3)), dma((2, 3, NCH, 3)), dma((NCH,)), dma((NCH,)),
     ]
     arrays = (ci, gi, go, taps, docs.reshape(4, 128), res, op, gain.reshape(1, 2048), ids.T, wts.T, wg, wu, wd)
     arrays = [pltpu.with_memory_space_constraint(v, pltpu.HBM) for v in arrays]

time: 73.9 us -> 72.3 us (0.978)
  Pallas kernels: 73 us -> 71.4 us
    pallas_call x1, Pallas kernels: 73 us -> 71.4 us  [on_device(): pl.pallas_call(layer_kernel, out_shape=jax.ShapeDtypeStruct((128, 2048),...]
where the time goes in v4:
time: 72.3 us; the launch traced here: 72.2 us
  Pallas kernels  71.4 us (99%)
  local copies, waits for them, and re-layouts  0.8 us (1%)
    pallas_call x1, Pallas kernels, on_device(): pl.pallas_call(layer_kernel, out_shape=jax.ShapeDtypeStruct((128, 2048),...  71.4 us

profile of v4, /device:TPU:1, one launch (start us, length us, event | category | flops | bytes accessed | tf_op | source)
XLA Modules:
  0.0 72.2 jit_solution(11360456044183164629)
XLA Ops:
  0.0 71.4 %shard_map.127 = bf16[128,2048]{1,0:T(8,128)(2,1)S(1)} custom-call(bf16[512,256]{1,0:T(8,128)(2,1)} %ci_h.1, bf16[512,256]{1,0:T(8,128)(2,1)} %gi_h.1, bf16[512,256]{1,0:T(8,128)(2,1)} %go_h.1, bf16[3,256]{1,0:T(4,128)(2,1)} %taps_h.1, s32[4,128]{1,0:T(4,128)} %bitcast.5, bf16[128,2048]{1,0:T(8,128)(2,1)} %res_h.1, bf16[1024,2048]{1,0:T(8,128)(2,1)} %op_h.1, ...), custom_call_target="tpu_custom_call" | custom-call | tf_op jit(solution)/shard_map/pallas_call | solution.py:417
  71.4 0.8 %copy.15 = bf16[128,2048]{1,0:T(8,128)(2,1)} copy(bf16[128,2048]{1,0:T(8,128)(2,1)S(1)} %shard_map.127) | data formatting | bytes 1048576

commit v5 on v4

--- a/solution.py
+++ b/solution.py
@@ -252,7 +252,7 @@
         return buf.at[(w, p, k, *index, slice(None), pl.ds(0, WIDTHS[k]))]
 
     def axis_of(w, p, k):
-        return (k + 2 * p + w) % 3
+        return (k + 2 * p + 2 * w) % 3
 
     def moves(buf, ss, rs, w, p, k, sign):
         axis = axis_of(w, p, k)

time: 72.3 us -> 73.7 us (1.019)
  Pallas kernels: 71.4 us -> 72.7 us
    pallas_call x1, Pallas kernels: 71.4 us -> 72.7 us  [on_device(): pl.pallas_call(layer_kernel, out_shape=jax.ShapeDtypeStruct((128, 2048),...]
where the time goes in v5:
time: 73.7 us; the launch traced here: 73.5 us
  Pallas kernels  72.7 us (99%)
  local copies, waits for them, and re-layouts  0.8 us (1%)
    pallas_call x1, Pallas kernels, on_device(): pl.pallas_call(layer_kernel, out_shape=jax.ShapeDtypeStruct((128, 2048),...  72.7 us

profile of v5, /device:TPU:1, one launch (start us, length us, event | category | flops | bytes accessed | tf_op | source)
XLA Modules:
  0.0 73.5 jit_solution(1874245408575765969)
XLA Ops:
  0.0 72.7 %shard_map.127 = bf16[128,2048]{1,0:T(8,128)(2,1)S(1)} custom-call(bf16[512,256]{1,0:T(8,128)(2,1)} %ci_h.1, bf16[512,256]{1,0:T(8,128)(2,1)} %gi_h.1, bf16[512,256]{1,0:T(8,128)(2,1)} %go_h.1, bf16[3,256]{1,0:T(4,128)(2,1)} %taps_h.1, s32[4,128]{1,0:T(4,128)} %bitcast.5, bf16[128,2048]{1,0:T(8,128)(2,1)} %res_h.1, bf16[1024,2048]{1,0:T(8,128)(2,1)} %op_h.1, ...), custom_call_target="tpu_custom_call" | custom-call | tf_op jit(solution)/shard_map/pallas_call | solution.py:417
  72.7 0.8 %copy.15 = bf16[128,2048]{1,0:T(8,128)(2,1)} copy(bf16[128,2048]{1,0:T(8,128)(2,1)S(1)} %shard_map.127) | data formatting | bytes 1048576
